TPU v7x, 32 devices: a whole 2x2x4 slice. The times are simulated.
32 devices in a mesh: grp: 2 (over y), sp: 4 (over z), tp: 4 (over x, core).
Axes of the slice: x: 2, y: 2, z: 4, core: 2. Of those that a mesh axis runs over, the one named last changes fastest.
Arguments:
- queries: bfloat16 [6144, 512], P(('grp', 'sp'), 'tp'), parts along dimension 0, may hold values from -6 to 6
- key_projected: bfloat16 [6144, 512], P(('grp', 'sp'), 'tp'), parts along dimension 0, may hold values from -6 to 6
- values: bfloat16 [6144, 1024], P(('grp', 'sp'), 'tp'), parts along dimension 0, may hold values from -6 to 6
- output_gate_preact: bfloat16 [6144, 1024], P(('grp', 'sp'), 'tp'), parts along dimension 0, may hold values from -6 to 6
- forward_decay_logits: bfloat16 [6144, 512], P(('grp', 'sp'), 'tp'), parts along dimension 0, may hold values from -3.8 to 3.8
- backward_decay_logits: bfloat16 [6144, 512], P(('grp', 'sp'), 'tp'), parts along dimension 0, may hold values from -3.8 to 3.8
- decay_logit_shift: float32 [2, 512], P(None, 'tp'), may hold values from -1 to 13
- decay_spike_values: float32 [8, 6144], P('tp', ('grp', 'sp')), parts along dimension 1, may hold values from -2.1 to 0
- residual: bfloat16 [6144, 2048], P(('grp', 'sp', 'tp')), parts along dimension 0, may hold values from -6 to 6
- head_norm_gain: float32 [1024], P('tp'), may hold values from 0.1 to 1.9
- output_projection: bfloat16 [1024, 2048], P('tp'), may hold values from -0.1875 to 0.1875
- prenorm_gain: float32 [2048], replicated, may hold values from 0.1 to 1.9
- gate_projection: bfloat16 [2048, 5120], P('sp', 'tp'), may hold values from -0.125 to 0.125
- up_projection: bfloat16 [2048, 5120], P('sp', 'tp'), may hold values from -0.125 to 0.125
- down_projection: bfloat16 [5120, 2048], P('tp', 'sp'), may hold values from -0.078125 to 0.078125
Outputs:
- layer_output: bfloat16 [6144, 2048], P(('grp', 'sp', 'tp')), parts along dimension 0
There are 2 independent parts, one for each index of `grp`. A program takes and returns all parts, laid end to end along the dimension named above; an argument that names none is the same for every part. Nothing has to cross between parts.
All inputs are finite; a program needn't handle non-finite values.
Results may differ from a plain program's by a relative error of at most 0.014.
Values may be sent and summed in bfloat16 or wider, within the bound.
A program may use at most 64 MiB of HBM per device.

v0:
```python
import functools

import jax
import jax.numpy as jnp
from jax import lax
from jax.experimental import pallas as pl
from jax.experimental.pallas import tpu as pltpu
from jax.sharding import PartitionSpec as P


KEY_CHANNELS = 64
HEAD_V = 128
BLOCK = 64
GATE_DENOMINATOR = 16.0
EPSILON = 1e-06
F32, BF16 = jnp.float32, jnp.bfloat16


def nt(a, b):
    return lax.dot_general(a, b, (((1,), (1,)), ((), ())), preferred_element_type=F32)


def tn(a, b):
    return lax.dot_general(a, b, (((0,), (0,)), ((), ())), preferred_element_type=F32)


def first_head(shape):
    return lax.broadcasted_iota(jnp.int32, shape, 1) < KEY_CHANNELS


VMEM = pl.BlockSpec(memory_space=pltpu.VMEM)


def cost(flops, size):
    return pl.CostEstimate(flops=flops, bytes_accessed=size, transcendentals=0)


def entering(value, axis, join, neutral, backward):
    count = lax.axis_size(axis)
    place = lax.axis_index(axis)
    ahead = count - 1 - place if backward else place
    gathered = jax.tree.map(
        lambda a, kind: lax.all_gather(a.astype(kind), axis), value, (jnp.bfloat16, jnp.bfloat16)
    )
    state = jax.tree.map(lambda a, e: jnp.zeros_like(a) + jnp.asarray(e, a.dtype), value, neutral)

    def one(lap, state):
        source = count - 1 - lap if backward else lap
        return join(
            state,
            jax.tree.map(
                lambda a, own: lax.dynamic_index_in_dim(a, source, 0, False).astype(own.dtype),
                gathered,
                value,
            ),
        )

    return lax.fori_loop(0, ahead, one, state)


def block_sweep(query_in, key_in, values_in, log_decay, span):
    sequence_length, head_count, key_dim = key_in.shape
    block_count = sequence_length // span

    def blocks(tensor):
        return jnp.transpose(
            tensor.reshape(block_count, span, head_count, tensor.shape[-1]), (0, 2, 1, 3)
        )

    lower_mask = jnp.tril(jnp.ones((span, span), dtype=bool))[:, :, None]

    def advance(carried, inputs):
        memory, offset = carried
        key_blk, value_blk, decay_blk, query_blk = inputs
        within = jnp.cumsum(decay_blk, axis=1)
        ending = within[:, -1, :]
        memory_next = jnp.exp(ending)[:, :, None] * memory + jnp.einsum(
            "hjd,hje->hde",
            key_blk * jnp.exp(ending[:, None, :] - within),
            value_blk,
            precision=lax.Precision.HIGHEST,
        )
        result = jnp.einsum(
            "hid,hde->hie", query_blk * jnp.exp(within), memory, precision=lax.Precision.HIGHEST
        )
        spread = jnp.exp(
            jnp.where(lower_mask, within[:, :, None, :] - within[:, None, :, :], -jnp.inf)
        )
        scores = jnp.einsum(
            "hid,hjd,hijd->hij", query_blk, key_blk, spread, precision=lax.Precision.HIGHEST
        )
        result = result + jnp.einsum(
            "hij,hje->hie", scores, value_blk, precision=lax.Precision.HIGHEST
        )
        reached = query_blk * jnp.exp(within + offset[:, None, :])
        return ((memory_next, offset + ending), (result, reached))

    start_memory = jnp.zeros((head_count, key_dim, values_in.shape[-1]), jnp.float32)
    start_offset = jnp.zeros((head_count, key_dim), jnp.float32)
    (memory, decay_total), (outputs, reached) = lax.scan(
        advance,
        (start_memory, start_offset),
        (blocks(key_in), blocks(values_in), blocks(log_decay), blocks(query_in)),
    )

    def unblock(tensor):
        return jnp.transpose(tensor, (0, 2, 1, 3)).reshape(
            sequence_length, head_count, tensor.shape[-1]
        )

    return (unblock(outputs), unblock(reached), memory, decay_total)


def head_mix(combined, head_norm_gain, output_gate_preact):
    sequence_length, head_count, width = combined.shape
    inverse = lax.rsqrt(jnp.mean(combined * combined, axis=-1, keepdims=True) + EPSILON)
    gate_act = jax.nn.silu(
        output_gate_preact.astype(jnp.float32).reshape(sequence_length, head_count, width)
    )
    weighted = combined * inverse * head_norm_gain.reshape(head_count, width) * gate_act
    return weighted.reshape(sequence_length, head_count * width).astype(jnp.bfloat16)


def row_norm(mid_rows, prenorm_gain):
    wide = mid_rows.astype(jnp.float32)
    inverse = lax.rsqrt(jnp.mean(wide * wide, axis=-1, keepdims=True) + EPSILON)
    return (wide * inverse * prenorm_gain).astype(jnp.bfloat16)


def combine_states(earlier, later):
    decay_early, memory_early = earlier
    decay_late, memory_late = later
    return (decay_early * decay_late, decay_late[:, :, None] * memory_early + memory_late)


def body(
    queries,
    key_projected,
    values,
    output_gate_preact,
    forward_decay_logits,
    backward_decay_logits,
    decay_logit_shift,
    decay_spike_values,
    residual,
    head_norm_gain,
    output_projection,
    prenorm_gain,
    gate_projection,
    up_projection,
    down_projection,
):
    sequence_length = queries.shape[0]
    local_heads = queries.shape[1] // KEY_CHANNELS
    query_f = queries.astype(jnp.float32).reshape(
        sequence_length, local_heads, KEY_CHANNELS
    ) * KEY_CHANNELS ** (-0.5)
    keys_f = key_projected.astype(jnp.float32).reshape(sequence_length, local_heads, KEY_CHANNELS)
    values_f = values.astype(jnp.float32).reshape(sequence_length, local_heads, HEAD_V)
    decay_spikes = jnp.transpose(decay_spike_values)[:, :, None]
    logit_shifts = decay_logit_shift.reshape(2, local_heads, KEY_CHANNELS)
    forward_decay = (
        jax.nn.log_sigmoid(
            forward_decay_logits.astype(jnp.float32).reshape(
                sequence_length, local_heads, KEY_CHANNELS
            )
            + logit_shifts[0]
        )
        / GATE_DENOMINATOR
        + decay_spikes
    )
    backward_decay = (
        jax.nn.log_sigmoid(
            backward_decay_logits.astype(jnp.float32).reshape(
                sequence_length, local_heads, KEY_CHANNELS
            )
            + logit_shifts[1]
        )
        / GATE_DENOMINATOR
        + decay_spikes
    )
    fwd_out, fwd_reach, fwd_memory, fwd_total = block_sweep(
        query_f, keys_f, values_f, forward_decay, BLOCK
    )
    bwd_out, bwd_reach, bwd_memory, bwd_total = block_sweep(
        query_f[::-1], keys_f[::-1], values_f[::-1], backward_decay[::-1], BLOCK
    )
    identity = (jnp.ones_like(fwd_total), jnp.zeros_like(fwd_memory))
    fwd_incoming = entering(
        (jnp.exp(fwd_total), fwd_memory), "sp", combine_states, identity, False
    )[1]
    bwd_incoming = entering((jnp.exp(bwd_total), bwd_memory), "sp", combine_states, identity, True)[
        1
    ]
    fwd_full = fwd_out + jnp.einsum(
        "lhd,hde->lhe", fwd_reach, fwd_incoming, precision=lax.Precision.HIGHEST
    )
    bwd_full = bwd_out + jnp.einsum(
        "lhd,hde->lhe", bwd_reach, bwd_incoming, precision=lax.Precision.HIGHEST
    )
    attended = head_mix(fwd_full + bwd_full[::-1], head_norm_gain, output_gate_preact)
    token_rows = lax.all_to_all(attended, "tp", split_axis=0, concat_axis=1, tiled=True)
    whole_out = lax.all_gather(output_projection, "tp", axis=0, tiled=True)
    projected = jnp.dot(token_rows, whole_out, preferred_element_type=jnp.float32)
    mid_rows = (residual.astype(jnp.float32) + projected).astype(jnp.bfloat16)
    normed = row_norm(mid_rows, prenorm_gain)
    fetched = (
        lax.all_gather(gate_projection, "sp", axis=0, tiled=True),
        lax.all_gather(up_projection, "sp", axis=0, tiled=True),
        lax.all_gather(down_projection, "sp", axis=1, tiled=True),
    )
    gate_full, up_full, down_full = fetched
    piece = lax.all_gather(normed, "tp", axis=0, tiled=True)
    gate_part = jnp.dot(piece, gate_full, preferred_element_type=jnp.float32)
    up_part = jnp.dot(piece, up_full, preferred_element_type=jnp.float32)
    hidden = (jax.nn.silu(gate_part) * up_part).astype(jnp.bfloat16)
    summed = lax.psum_scatter(
        jnp.dot(hidden, down_full, preferred_element_type=jnp.float32).astype(jnp.bfloat16),
        "tp",
        scatter_dimension=0,
        tiled=True,
    ).astype(jnp.float32)
    return (mid_rows.astype(jnp.float32) + 0.5 * summed).astype(jnp.bfloat16)


MESH = pl.DeviceIdType.MESH
PIECES = 5


def log_decay(logits, shift, spike):
    x = logits.astype(F32) + shift
    soft = jnp.minimum(x, 0.0) - jnp.log1p(jnp.exp(-jnp.abs(x)))
    return soft / GATE_DENOMINATOR + spike


def own_states(k_ref, v_ref, fd_ref, bd_ref, shift_ref, spike_ref, within_ref, kd_ref, fwd_ref, bwd_ref):
    tokens, lanes = k_ref.shape
    blocks = tokens // BLOCK
    row = lax.broadcasted_iota(jnp.int32, (2 * BLOCK, 2 * BLOCK), 0)
    col = lax.broadcasted_iota(jnp.int32, (2 * BLOCK, 2 * BLOCK), 1)
    r, c = row % BLOCK, col % BLOCK
    ahead = jnp.where(row < BLOCK, r - c, c - r)
    tri = jnp.where(ahead >= 0, 1.0, 0.0).astype(BF16)
    half = first_head((BLOCK, lanes))
    ends = []
    for b in range(blocks):
        at = slice(b * BLOCK, (b + 1) * BLOCK)
        spike = jnp.where(half, spike_ref[at, 0:1], spike_ref[at, 1:2])
        parts = [log_decay(ref[at, :], shift_ref[n : n + 1, :], spike) for n, ref in enumerate((fd_ref, bd_ref))]
        d = jnp.concatenate(parts, axis=1)
        hi = d.astype(BF16)
        lo = (d - hi.astype(F32)).astype(BF16)
        both = jnp.dot(tri, jnp.concatenate([hi, lo], axis=0), preferred_element_type=F32)
        fwd, bwd = both[:BLOCK, :lanes], both[BLOCK:, lanes:]
        within_ref[at, :lanes] = fwd
        within_ref[at, lanes:] = bwd
        ends.append((fwd[BLOCK - 1 :, :], bwd[:1, :]))
    zero = jnp.zeros((1, lanes), F32)
    after, before = [zero] * blocks, [zero] * blocks
    for b in range(1, blocks):
        before[b] = before[b - 1] + ends[b - 1][1]
        after[blocks - 1 - b] = after[blocks - b] + ends[blocks - b][0]
    totals = after[0] + ends[0][0], before[-1] + ends[-1][1]
    for b in range(blocks):
        at = slice(b * BLOCK, (b + 1) * BLOCK)
        key = k_ref[at, :].astype(F32)
        kd_ref[at, :lanes] = (key * jnp.exp((ends[b][0] + after[b]) - within_ref[at, :lanes])).astype(BF16)
        kd_ref[at, lanes:] = (key * jnp.exp((ends[b][1] + before[b]) - within_ref[at, lanes:])).astype(BF16)
    full = tn(v_ref[...], kd_ref[...])
    mine = first_head((HEAD_V, lanes))
    for n, ref in enumerate((fwd_ref, bwd_ref)):
        u = full[:, n * lanes : (n + 1) * lanes]
        ref[:HEAD_V, :] = jnp.where(mine, u[:HEAD_V], u[HEAD_V:]).astype(BF16)
        ref[HEAD_V:, :] = jnp.broadcast_to(jnp.exp(totals[n]), (16, lanes)).astype(BF16)


def spread(state):
    mine = first_head(state.shape)
    return jnp.concatenate([jnp.where(mine, state, 0.0), jnp.where(mine, 0.0, state)], axis=0).astype(BF16)


def pack(u):
    top = u[:HEAD_V]
    return jnp.where(first_head(top.shape), top, u[HEAD_V:])


def backward_states(k_ref, v_ref, within_ref, state, held_ref):
    tokens, lanes = k_ref.shape
    for b in reversed(range(tokens // BLOCK)):
        at = slice(b * BLOCK, (b + 1) * BLOCK)
        held_ref[b] = spread(state)
        within = within_ref[at, lanes:]
        end = within[:1, :]
        kd = (k_ref[at, :].astype(F32) * jnp.exp(end - within)).astype(BF16)
        state = state * jnp.exp(end) + pack(tn(v_ref[at, :], kd))


def attend(q_ref, k_ref, v_ref, within_ref, gate_ref, gain_ref, fwd_state, held_ref, out_ref):
    tokens, lanes = k_ref.shape
    row = lax.broadcasted_iota(jnp.int32, (2 * BLOCK, BLOCK), 0) % BLOCK
    col = lax.broadcasted_iota(jnp.int32, (2 * BLOCK, BLOCK), 1)
    half = first_head((BLOCK, lanes))
    for b in range(tokens // BLOCK):
        at = slice(b * BLOCK, (b + 1) * BLOCK)
        query = q_ref[at, :].astype(F32) * KEY_CHANNELS ** (-0.5)
        key = k_ref[at, :].astype(F32)
        value = v_ref[at, :]
        scores, reach = [], []
        for n in range(2):
            within = within_ref[at, n * lanes : (n + 1) * lanes]
            pivot = within[BLOCK // 2 - 1 + n : BLOCK // 2 + n, :]
            near = (query * jnp.exp(within - pivot)).astype(BF16)
            far = (key * jnp.exp(pivot - within)).astype(BF16)
            zero = jnp.zeros_like(near)
            pair = jnp.concatenate([jnp.where(half, near, zero), jnp.where(half, zero, near)], axis=0)
            scores.append(nt(pair, far))
            reach.append((query * jnp.exp(within)).astype(BF16))
        score = (jnp.where(col <= row, scores[0], 0.0) + jnp.where(col >= row, scores[1], 0.0)).astype(BF16)
        states = jnp.concatenate([spread(fwd_state), held_ref[b]], axis=1)
        result = nt(jnp.concatenate(reach, axis=1), states)
        for h in range(2):
            lane = slice(h * HEAD_V, (h + 1) * HEAD_V)
            x = result[:, lane] + jnp.dot(
                score[h * BLOCK : (h + 1) * BLOCK], value[:, lane], preferred_element_type=F32
            )
            inverse = lax.rsqrt(jnp.mean(x * x, axis=-1, keepdims=True) + EPSILON)
            g = gate_ref[at, lane].astype(F32)
            out_ref[at, lane] = (x * inverse * gain_ref[:, lane] * (g * jax.nn.sigmoid(g))).astype(BF16)
        within = within_ref[at, :lanes]
        end = within[BLOCK - 1 :, :]
        kd = (key * jnp.exp(end - within)).astype(BF16)
        fwd_state = fwd_state * jnp.exp(end) + pack(tn(value, kd))


def pick(i, table):
    value = table[0]
    for n, item in enumerate(table[1:], 1):
        value = jnp.where(i == n, item, value)
    return value


def ds(first, size):
    return pl.ds(pl.multiple_of(first, size if size % 128 == 0 else 16), size)


def layer_kernel(
    k_ref, v_ref, fd_ref, bd_ref, shift_ref, spike_ref, q_ref, gate_ref, gain_ref, norm_ref,
    res_hbm, out_hbm, g_hbm, u_hbm, d_hbm,
    out_ref,
    within, kd, fown, bown, fgot, bgot, fstate, bstate, held, attended, rows, outw, res, mid, acts,
    wg, wu, wd, hid, part, got, xsend, xgot, esend, egot, erelay,
    loc, st_s, st_r, a2a_s, a2a_r, ow_s, ow_r, ag_s, ag_r, ea_s, gs, gr, dsd, drv, cr_s, cr_r, xo_s, xo_r,
    eo_s, eo_r, er_s, er_r,
):
    count = lax.axis_size("sp")
    side, place, me = lax.axis_index("grp"), lax.axis_index("sp"), lax.axis_index("tp")
    chip, core = me // 2, me % 2
    tc, tx, td = 2 * chip + 1 - core, 2 * (1 - chip) + core, 2 * (1 - chip) + 1 - core
    upper = place // 2
    e, m, o, oe = 3 * upper, 1 + upper, 2 - upper, 3 - 3 * upper
    middle = place * (count - 1 - place) > 0
    own = res.shape[0]
    width = attended.shape[1]
    model = mid.shape[1]
    depth, hidden = g_hbm.shape
    tile = hidden // PIECES
    hr = depth // 2
    dr = hidden // 4
    dw = d_hbm.shape[1]
    orow = width // 4
    nrow = own // 2

    def remote(src, dst, send, recv, **dev):
        return pltpu.make_async_remote_copy(
            src_ref=src, dst_ref=dst, send_sem=send, recv_sem=recv, device_id=dev, device_id_type=MESH
        )

    def gu(n, source, half, p, local=False, **dev):
        dst = (wg, wu)[n].at[p, ds(source * depth + half * hr, hr), :]
        src = (g_hbm, u_hbm)[n].at[ds(half * hr, hr), ds(p * tile, tile)] if local else dst
        return remote(src, dst, gs.at[n, source, half, p], gr.at[n, source, half, p], **(dev or dict(sp=o)))

    def dn(source, half, p, local=False, **dev):
        at = ds(half * 2 * dr + p * dr, dr)
        dst = wd.at[source, at, :]
        src = d_hbm.at[at, :] if local else dst
        return remote(src, dst, dsd.at[source, half, p], drv.at[source, half, p], **(dev or dict(sp=o)))

    def send_gu(source, half, p, local=False, **dev):
        for n in range(2):
            gu(n, source, half, p, local, **dev).start()

    def take_gu(source, half, p):
        for n in range(2):
            gu(n, source, half, p).wait_recv()

    def relay_gu(source, p, **dev):
        take_gu(source, side, p)
        send_gu(source, side, p, **dev)

    def relay_dn(source, p, **dev):
        dn(source, side, p).wait_recv()
        dn(source, side, p, **dev).start()

    def ow(kind, block, i, dev, local=False):
        dst = outw.at[ds(block * width + i * orow, orow), :]
        src = out_hbm.at[i * orow : (i + 1) * orow, :] if local else dst
        return remote(src, dst, ow_s.at[kind, i], ow_r.at[block, i], tp=dev)

    def relay_ow(i):
        ow(2, tx, i, tc).wait_recv()
        ow(2, tx, i, tc).start()

    def a2a(n, block, dev):
        return remote(
            attended.at[ds(dev * own, own), :], rows.at[:, ds(block * width, width)], a2a_s.at[n], a2a_r.at[block], tp=dev
        )

    def ag(q, kind, block, i, dev):
        at = acts.at[q, ds(block * own + i * nrow, nrow), :]
        return remote(at, at, ag_s.at[q, kind, i], ag_r.at[q, block, i], tp=dev)

    def to_host(i):
        at = ds(me * own + i * nrow, nrow)
        return remote(acts.at[0, at, :], acts.at[1, at, :], ea_s.at[i], ag_r.at[1, me, i], sp=m)

    def state_copy(n, k, dev):
        src, dst = ((fown, fgot), (bown, bgot))[n]
        return remote(src, dst.at[k - 1], st_s.at[n, k - 1], st_r.at[n, k - 1], sp=dev)

    def cr(q, i, j):
        block = 2 * j + 1 - core
        return remote(part.at[q, i, ds(block * own, own), :], got.at[q, i, j], cr_s.at[q, i, j], cr_r.at[q, i, j], tp=tc)

    def xo(i):
        return remote(xsend.at[i], xgot.at[i], xo_s.at[i], xo_r.at[i], tp=tx)

    def eo(i, n):
        dst = egot.at[0, i] if n == 0 else erelay.at[i]
        return remote(esend.at[i, n], dst, eo_s.at[i, n], eo_r.at[i, n], sp=e)

    def er(i):
        return remote(erelay.at[i], egot.at[1, i], er_s.at[i], er_r.at[i], tp=tx)

    own_copies = []
    for p in range(PIECES):
        for n in range(2):
            own_copies.append(
                pltpu.make_async_copy(
                    (g_hbm, u_hbm)[n].at[:, p * tile : (p + 1) * tile],
                    (wg, wu)[n].at[p, ds(place * depth, depth), :],
                    loc.at[n * PIECES + p],
                )
            )
    own_copies.append(pltpu.make_async_copy(d_hbm, wd.at[place], loc.at[2 * PIECES]))
    own_out = pltpu.make_async_copy(out_hbm, outw.at[ds(me * width, width), :], loc.at[2 * PIECES + 1])
    own_res = pltpu.make_async_copy(res_hbm, res, loc.at[2 * PIECES + 2])

    barrier = pltpu.get_barrier_semaphore()
    friends = [dict(sp=lax.rem(place + k, count)) for k in range(1, count)]
    friends += [dict(grp=1 - side)] + [dict(tp=t) for t in (tc, tx, td)]
    for friend in friends:
        pl.semaphore_signal(barrier, inc=1, device_id=friend, device_id_type=MESH)
    pl.semaphore_wait(barrier, len(friends))

    @pl.when(middle)
    def _():
        send_gu(place, side, 0, True, sp=o)

    @pl.when(jnp.logical_not(middle))
    def _():
        send_gu(place, side, 0, True, sp=m)

    for i in range(4):
        ow(0, me, i, tx, True).start()
    for i in range(4):
        ow(1, me, i, tc, True).start()
    own_out.start()
    own_res.start()

    own_states(k_ref, v_ref, fd_ref, bd_ref, shift_ref, spike_ref, within, kd, fown, bown)
    for k in range(1, count):

        @pl.when(place + k < count)
        def _(k=k):
            state_copy(0, k, place + k).start()

        @pl.when(place >= k)
        def _(k=k):
            state_copy(1, k, place - k).start()

    @pl.when(middle)
    def _():
        for copy in own_copies:
            copy.start()
        for p in range(1, PIECES):
            send_gu(place, side, p, True, sp=o)
        relay_gu(o, 0, grp=1 - side)

    @pl.when(jnp.logical_not(middle))
    def _():
        for p in range(1, PIECES):
            send_gu(place, side, p, True, sp=m)

    fstate[...] = jnp.zeros_like(fstate)
    bstate[...] = jnp.zeros_like(bstate)
    for k in reversed(range(1, count)):

        @pl.when(place >= k)
        def _(k=k):
            state_copy(0, k, place).wait_recv()
            decay = fgot[k - 1, HEAD_V : HEAD_V + 1, :].astype(F32)
            fstate[...] = fstate[...] * decay + fgot[k - 1, :HEAD_V, :].astype(F32)

        @pl.when(place + k < count)
        def _(k=k):
            state_copy(1, k, place).wait_recv()
            decay = bgot[k - 1, HEAD_V : HEAD_V + 1, :].astype(F32)
            bstate[...] = bstate[...] * decay + bgot[k - 1, :HEAD_V, :].astype(F32)

    relay_ow(0)
    backward_states(k_ref, v_ref, within, bstate[...], held)

    @pl.when(middle)
    def _():
        relay_gu(o, 1, grp=1 - side)

    relay_ow(1)
    attend(q_ref, k_ref, v_ref, within, gate_ref, gain_ref, fstate[...], held, attended)
    others = (tx, td, tc)
    for n, t in enumerate(others):
        a2a(n, me, t).start()
    rows[:, ds(me * width, width)] = attended[ds(me * own, own), :]

    @pl.when(middle)
    def _():
        relay_gu(e, 0, sp=o)
        relay_gu(e, 1, sp=o)
        relay_gu(o, 2, grp=1 - side)

    relay_ow(2)

    @pl.when(middle)
    def _():
        relay_gu(e, 2, sp=o)
        relay_gu(o, 3, grp=1 - side)
        relay_gu(e, 3, sp=o)

    relay_ow(3)
    for t in others:
        a2a(0, t, t).wait_recv()
    for t in (tc, td):
        for i in range(4):
            ow(0, t, i, tc).wait_recv()
    own_out.wait()
    own_res.wait()

    total = jnp.zeros((own, 1), F32)
    wide = 512
    for n in range(model // wide):
        at = slice(n * wide, (n + 1) * wide)
        projected = jnp.dot(rows[...], outw[:, at], preferred_element_type=F32)
        mixed = (res[:, at].astype(F32) + projected).astype(BF16)
        mid[:, at] = mixed
        mixed = mixed.astype(F32)
        total += jnp.sum(mixed * mixed, axis=-1, keepdims=True)
    inverse = lax.rsqrt(total / model + EPSILON)
    for n in range(model // wide):
        at = slice(n * wide, (n + 1) * wide)
        acts[0, ds(me * own, own), at] = (mid[:, at].astype(F32) * inverse * norm_ref[:, at]).astype(BF16)

    def target(i):
        return pick(i, (m, o, oe, e))

    @pl.when(middle)
    def _():
        for i in range(2):
            ag(0, 0, me, i, tx).start()
            ag(0, 1, me, i, tc).start()
        relay_gu(o, 4, grp=1 - side)
        relay_gu(e, 4, sp=o)
        for p in range(2):
            dn(place, side, p, True, sp=o).start()
        for copy in own_copies:
            copy.wait()

        def relay_own(i):
            ag(0, 2, tx, i, tc).wait_recv()
            ag(0, 2, tx, i, tc).start()

        def relay_hosted(i):
            ag(1, 0, me, i, tx).wait_recv()
            ag(1, 0, me, i, tx).start()
            ag(1, 1, me, i, tc).start()

        relay_gu(oe, 0, grp=1 - side)
        relay_own(0)
        relay_gu(oe, 1, grp=1 - side)
        relay_hosted(0)
        relay_gu(oe, 2, grp=1 - side)
        relay_own(1)
        relay_hosted(1)
        relay_gu(oe, 3, grp=1 - side)

        order = [(0, 0), (0, 1), (0, 2), (1, 0), (0, 3), (1, 1), (0, 4), (1, 2), (1, 3), (1, 4)]

        def first(i, carry):
            q, j = pick(i, [a for a, _ in order]), pick(i, [b for _, b in order])

            @pl.when(i == 0)
            def _():
                for t in (tc, td):
                    for n in range(2):
                        ag(0, 0, t, n, tc).wait_recv()

            @pl.when(i == 1)
            def _():
                relay_gu(oe, 4, grp=1 - side)

            for n in range(2):

                @pl.when(i == 2 + n)
                def _(n=n):
                    ag(1, 2, tx, n, tc).wait_recv()
                    ag(1, 2, tx, n, tc).start()

            @pl.when(i == 3)
            def _():
                for t in (tc, td):
                    for n in range(2):
                        ag(1, 0, t, n, tc).wait_recv()

            for n in range(2):

                @pl.when(i == 5 + n)
                def _(n=n):
                    relay_dn(o, n, grp=1 - side)

            @pl.when(q == 0)
            def _():
                for source in (o, oe, e):
                    take_gu(source, 1 - side, j)

            g = jnp.dot(acts[q], wg[j], preferred_element_type=F32)
            u = jnp.dot(acts[q], wu[j], preferred_element_type=F32)
            hid[q, :, ds(j * tile, tile)] = (g * jax.nn.sigmoid(g) * u).astype(BF16)
            return carry

        lax.fori_loop(0, len(order), first, 0)

        def fold(i, q):
            for j in range(2):
                cr(q, i, j).wait_recv()

            def both(block, j):
                return part[q, i, ds(block * own, own), :].astype(F32) + got[q, i, j].astype(F32)

            @pl.when(q == 0)
            def _():
                xsend[i] = both(tx, 1 - chip).astype(BF16)
                xo(i).start()

            @pl.when(q == 1)
            def _():
                esend[i, 0] = both(me, chip).astype(BF16)
                eo(i, 0).start()
                esend[i, 1] = both(tx, 1 - chip).astype(BF16)
                eo(i, 1).start()

        def second(s, carry):
            i, q = s // 2, s % 2

            @pl.when(s == 2)
            def _():
                relay_dn(e, 0, sp=o)
                for p in range(2):
                    dn(o, 1 - side, p).wait_recv()

            @pl.when(s == 3)
            def _():
                relay_dn(e, 1, sp=o)
                relay_dn(oe, 0, grp=1 - side)

            @pl.when(s == 4)
            def _():
                relay_dn(oe, 1, grp=1 - side)
                for p in range(2):
                    dn(oe, 1 - side, p).wait_recv()

            @pl.when(s == 6)
            def _():
                for p in range(2):
                    dn(e, 1 - side, p).wait_recv()

            part[q, i] = jnp.dot(hid[q], wd[target(i)], preferred_element_type=F32).astype(BF16)
            for j in range(2):
                cr(q, i, j).start()

            @pl.when(s > 0)
            def _():
                fold((s - 1) // 2, (s + 1) % 2)

            return carry

        lax.fori_loop(0, 2 * count, second, 0)
        fold(count - 1, 1)

        for i in range(count):
            xo(i).wait_recv()
            at = ds(target(i) * dw, dw)
            total = part[0, i, ds(me * own, own), :].astype(F32) + got[0, i, chip].astype(F32) + xgot[i].astype(F32)
            out_ref[:, at] = (mid[:, at].astype(F32) + 0.5 * total).astype(BF16)

        for p in range(PIECES):
            for n in range(2):
                gu(n, place, side, p, True).wait_send()
                for source in (e, o, oe):
                    gu(n, source, side, p).wait_send()
        for p in range(2):
            dn(place, side, p, True).wait_send()
            for source in (e, o, oe):
                dn(source, side, p).wait_send()
        for q in range(2):
            for kind in range(3):
                for i in range(2):
                    ag(q, kind, me, i, tc).wait_send()
            for i in range(count):
                for j in range(2):
                    cr(q, i, j).wait_send()
        for i in range(count):
            xo(i).wait_send()
            for n in range(2):
                eo(i, n).wait_send()

    @pl.when(jnp.logical_not(middle))
    def _():
        for i in range(2):
            to_host(i).start()
        for p in range(PIECES):
            send_gu(place, 1 - side, p, True, sp=m)
        for half in (side, 1 - side):
            for p in range(2):
                dn(place, half, p, True, sp=m).start()
        for i in range(count):
            eo(i, 1).wait_recv()
            er(i).start()
        for i in range(count):
            eo(i, 0).wait_recv()
            er(i).wait_recv()
            at = ds(target(i) * dw, dw)
            total = egot[0, i].astype(F32) + egot[1, i].astype(F32)
            out_ref[:, at] = (mid[:, at].astype(F32) + 0.5 * total).astype(BF16)
        for i in range(2):
            to_host(i).wait_send()
        for half in (side, 1 - side):
            for p in range(PIECES):
                for n in range(2):
                    gu(n, place, half, p, True).wait_send()
            for p in range(2):
                dn(place, half, p, True).wait_send()
        for i in range(count):
            er(i).wait_send()

    for k in range(1, count):

        @pl.when(place + k < count)
        def _(k=k):
            state_copy(0, k, place).wait_send()

        @pl.when(place >= k)
        def _(k=k):
            state_copy(1, k, place).wait_send()

    for n, t in enumerate(others):
        a2a(n, me, t).wait_send()
    for kind in range(3):
        for i in range(4):
            ow(kind, me, i, tc).wait_send()


def fast_body(
    queries,
    key_projected,
    values,
    output_gate_preact,
    forward_decay_logits,
    backward_decay_logits,
    decay_logit_shift,
    decay_spike_values,
    residual,
    head_norm_gain,
    output_projection,
    prenorm_gain,
    gate_projection,
    up_projection,
    down_projection,
):
    count = lax.axis_size("sp")
    tokens, lanes = queries.shape
    width = values.shape[1]
    own, model = residual.shape
    depth, hidden = gate_projection.shape
    dw = down_projection.shape[1]
    tps = tokens // own
    blocks = tokens // BLOCK
    dma = lambda *shape: pltpu.SemaphoreType.DMA(shape)
    state = (HEAD_V + 16, lanes)
    V = pltpu.VMEM
    scratch = [
        V((tokens, 2 * lanes), F32),
        V((tokens, 2 * lanes), BF16),
        V(state, BF16),
        V(state, BF16),
        V((count - 1,) + state, BF16),
        V((count - 1,) + state, BF16),
        V((HEAD_V, lanes), F32),
        V((HEAD_V, lanes), F32),
        V((blocks, 2 * HEAD_V, lanes), BF16),
        V((tokens, width), BF16),
        V((own, tps * width), BF16),
        V((tps * width, model), BF16),
        V((own, model), BF16),
        V((own, model), BF16),
        V((2, tokens, model), BF16),
        V((PIECES, model, hidden // PIECES), BF16),
        V((PIECES, model, hidden // PIECES), BF16),
        V((count, hidden, dw), BF16),
        V((2, tokens, hidden), BF16),
        V((2, count, tokens, dw), BF16),
        V((2, count, 2, own, dw), BF16),
        V((count, own, dw), BF16),
        V((count, own, dw), BF16),
        V((count, 2, own, dw), BF16),
        V((2, count, own, dw), BF16),
        V((count, own, dw), BF16),
        dma(2 * PIECES + 3),
        dma(2, count - 1),
        dma(2, count - 1),
        dma(3),
        dma(tps),
        dma(3, 4),
        dma(tps, 4),
        dma(2, 3, 2),
        dma(2, tps, 2),
        dma(2),
        dma(2, count, 2, PIECES),
        dma(2, count, 2, PIECES),
        dma(count, 2, 2),
        dma(count, 2, 2),
        dma(2, count, 2),
        dma(2, count, 2),
        dma(count),
        dma(count),
        dma(count, 2),
        dma(count, 2),
        dma(count),
        dma(count),
    ]
    anywhere = pl.BlockSpec(memory_space=pl.ANY)
    return pl.pallas_call(
        layer_kernel,
        out_shape=jax.ShapeDtypeStruct((own, model), BF16),
        in_specs=[VMEM] * 10 + [anywhere] * 5,
        out_specs=VMEM,
        scratch_shapes=scratch,
        compiler_params=pltpu.CompilerParams(
            collective_id=0, has_side_effects=True, vmem_limit_bytes=67043328
        ),
        cost_estimate=cost(3 * 10**10, 3 * 10**7),
        name="layer",
    )(
        key_projected,
        values,
        forward_decay_logits,
        backward_decay_logits,
        decay_logit_shift,
        jnp.transpose(decay_spike_values),
        queries,
        output_gate_preact,
        head_norm_gain[None, :],
        prenorm_gain[None, :],
        residual,
        output_projection,
        gate_projection,
        up_projection,
        down_projection,
    )


def solution(mesh):
    in_specs = (
        P(("grp", "sp"), "tp"),
        P(("grp", "sp"), "tp"),
        P(("grp", "sp"), "tp"),
        P(("grp", "sp"), "tp"),
        P(("grp", "sp"), "tp"),
        P(("grp", "sp"), "tp"),
        P(None, "tp"),
        P("tp", ("grp", "sp")),
        P(("grp", "sp", "tp"), None),
        P("tp"),
        P("tp", None),
        P(),
        P("sp", "tp"),
        P("sp", "tp"),
        P("tp", "sp"),
    )
    out_specs = P(("grp", "sp", "tp"), None)

    def run(*args):
        lanes = args[0].shape[1]
        sizes = (mesh.shape["grp"], mesh.shape["sp"], mesh.shape["tp"])
        fits = lanes == 2 * KEY_CHANNELS and sizes == (2, 4, 4)
        return fast_body(*args) if fits else body(*args)

    return jax.shard_map(run, mesh=mesh, in_specs=in_specs, out_specs=out_specs, check_vma=False)
```

profile of v0, /device:TPU:0, one launch (start us, length us, event | category | flops | bytes accessed | tf_op | source)
XLA Modules:
  0.0 159.7 jit_solution(2989273668879089838)
XLA Ops:
  0.0 1.6 %copy.16 = f32[2,768]{0,1:T(8,128)} copy(f32[2,768]{1,0:T(2,128)} %param.22) | data formatting | bytes 12288 | tf_op args[7]
  1.6 156.0 %layer.1 = bf16[192,2048]{1,0:T(8,128)(2,1)} custom-call(bf16[768,128]{1,0:T(8,128)(2,1)} %k_ref.1, bf16[768,256]{1,0:T(8,128)(2,1)} %v_ref.1, bf16[768,128]{1,0:T(8,128)(2,1)} %fd_ref.1, bf16[768,128]{1,0:T(8,128)(2,1)} %bd_ref.1, f32[2,128]{1,0:T(2,128)} %shift_ref.1, f32[768,2]{1,0:T(8,128)} %bitcast.3, bf16[768,128]{1,0:T(8,128)(2,1)} %q_ref.1, ...), custom_call_target="tpu_custom_call" | custom-call | flops 30000001024 | bytes 30000000 | tf_op jit(solution)/shard_map/layer/pallas_call | solution.py:860
  157.6 2.1 %copy.18 = bf16[192,2048]{1,0:T(8,128)(2,1)} copy(bf16[192,2048]{1,0:T(8,128)(2,1)} %layer.1) | data formatting | bytes 1572864
where the time goes:
time: 160 us
  Pallas kernels  156 us (98%)
  local copies, waits for them, and re-layouts  3.71 us (2%)
    pallas_call x1, Pallas kernels, fast_body(): pl.pallas_call(layer_kernel, out_shape=jax.ShapeDtypeStruct((own, model),...  156 us
    unnamed x2, local copies, waits for them, and re-layouts  3.71 us

commit v1 on v0

--- a/solution.py
+++ b/solution.py
@@ -242,10 +242,11 @@
     ahead = jnp.where(row < BLOCK, r - c, c - r)
     tri = jnp.where(ahead >= 0, 1.0, 0.0).astype(BF16)
     half = first_head((BLOCK, lanes))
+    spikes = jnp.transpose(jnp.concatenate([spike_ref[...]] * 4, axis=0))
     ends = []
     for b in range(blocks):
         at = slice(b * BLOCK, (b + 1) * BLOCK)
-        spike = jnp.where(half, spike_ref[at, 0:1], spike_ref[at, 1:2])
+        spike = jnp.where(half, spikes[at, 0:1], spikes[at, 1:2])
         parts = [log_decay(ref[at, :], shift_ref[n : n + 1, :], spike) for n, ref in enumerate((fd_ref, bd_ref))]
         d = jnp.concatenate(parts, axis=1)
         hi = d.astype(BF16)
@@ -359,14 +360,16 @@
     upper = place // 2
     e, m, o, oe = 3 * upper, 1 + upper, 2 - upper, 3 - 3 * upper
     middle = place * (count - 1 - place) > 0
+    outer = jnp.logical_not(middle)
     own = res.shape[0]
     width = attended.shape[1]
     model = mid.shape[1]
     depth, hidden = g_hbm.shape
     tile = hidden // PIECES
     hr = depth // 2
-    dr = hidden // 4
-    dw = d_hbm.shape[1]
+    dr = hidden // 2
+    dw = wd.shape[3]
+    chunks = part.shape[1]
     orow = width // 4
     nrow = own // 2
 
@@ -375,20 +378,20 @@
             src_ref=src, dst_ref=dst, send_sem=send, recv_sem=recv, device_id=dev, device_id_type=MESH
         )
 
-    def gu(n, source, half, p, local=False, **dev):
+    def gu(n, source, half, p, local=False, again=False, **dev):
         dst = (wg, wu)[n].at[p, ds(source * depth + half * hr, hr), :]
         src = (g_hbm, u_hbm)[n].at[ds(half * hr, hr), ds(p * tile, tile)] if local else dst
-        return remote(src, dst, gs.at[n, source, half, p], gr.at[n, source, half, p], **(dev or dict(sp=o)))
+        send = gs.at[n, source, 1 - half if again else half, p]
+        return remote(src, dst, send, gr.at[n, source, half, p], **(dev or dict(sp=o)))
 
     def dn(source, half, p, local=False, **dev):
-        at = ds(half * 2 * dr + p * dr, dr)
-        dst = wd.at[source, at, :]
-        src = d_hbm.at[at, :] if local else dst
+        dst = wd.at[source, p, ds(half * dr, dr), :]
+        src = d_hbm.at[ds(half * dr, dr), p * dw : (p + 1) * dw] if local else dst
         return remote(src, dst, dsd.at[source, half, p], drv.at[source, half, p], **(dev or dict(sp=o)))
 
-    def send_gu(source, half, p, local=False, **dev):
+    def send_gu(source, half, p, local=False, again=False, **dev):
         for n in range(2):
-            gu(n, source, half, p, local, **dev).start()
+            gu(n, source, half, p, local, again, **dev).start()
 
     def take_gu(source, half, p):
         for n in range(2):
@@ -398,8 +401,11 @@
         take_gu(source, side, p)
         send_gu(source, side, p, **dev)
 
+    def take_dn(source, half, p):
+        dn(source, half, p).wait_recv()
+
     def relay_dn(source, p, **dev):
-        dn(source, side, p).wait_recv()
+        take_dn(source, side, p)
         dn(source, side, p, **dev).start()
 
     def ow(kind, block, i, dev, local=False):
@@ -432,8 +438,8 @@
         block = 2 * j + 1 - core
         return remote(part.at[q, i, ds(block * own, own), :], got.at[q, i, j], cr_s.at[q, i, j], cr_r.at[q, i, j], tp=tc)
 
-    def xo(i):
-        return remote(xsend.at[i], xgot.at[i], xo_s.at[i], xo_r.at[i], tp=tx)
+    def xo(q, i):
+        return remote(xsend.at[q, i], xgot.at[q, i], xo_s.at[q, i], xo_r.at[q, i], tp=tx)
 
     def eo(i, n):
         dst = egot.at[0, i] if n == 0 else erelay.at[i]
@@ -452,24 +458,41 @@
                     loc.at[n * PIECES + p],
                 )
             )
-    own_copies.append(pltpu.make_async_copy(d_hbm, wd.at[place], loc.at[2 * PIECES]))
-    own_out = pltpu.make_async_copy(out_hbm, outw.at[ds(me * width, width), :], loc.at[2 * PIECES + 1])
-    own_res = pltpu.make_async_copy(res_hbm, res, loc.at[2 * PIECES + 2])
+    for p in range(2):
+        own_copies.append(
+            pltpu.make_async_copy(d_hbm.at[:, p * dw : (p + 1) * dw], wd.at[place, p], loc.at[2 * PIECES + p])
+        )
+    own_out = pltpu.make_async_copy(out_hbm, outw.at[ds(me * width, width), :], loc.at[2 * PIECES + 2])
+    own_res = pltpu.make_async_copy(res_hbm, res, loc.at[2 * PIECES + 3])
 
     barrier = pltpu.get_barrier_semaphore()
     friends = [dict(sp=lax.rem(place + k, count)) for k in range(1, count)]
     friends += [dict(grp=1 - side)] + [dict(tp=t) for t in (tc, tx, td)]
     for friend in friends:
         pl.semaphore_signal(barrier, inc=1, device_id=friend, device_id_type=MESH)
+    own_states(k_ref, v_ref, fd_ref, bd_ref, shift_ref, spike_ref, within, kd, fown, bown)
     pl.semaphore_wait(barrier, len(friends))
+
+    for k in range(1, count):
+
+        @pl.when(place + k < count)
+        def _(k=k):
+            state_copy(0, k, place + k).start()
+
+        @pl.when(place >= k)
+        def _(k=k):
+            state_copy(1, k, place - k).start()
 
     @pl.when(middle)
     def _():
-        send_gu(place, side, 0, True, sp=o)
-
-    @pl.when(jnp.logical_not(middle))
+        for p in range(PIECES):
+            send_gu(place, side, p, True, sp=o)
+
+    @pl.when(outer)
     def _():
-        send_gu(place, side, 0, True, sp=m)
+        for p in range(PIECES):
+            send_gu(place, side, p, True, sp=m)
+        send_gu(place, 1 - side, 0, True, sp=m)
 
     for i in range(4):
         ow(0, me, i, tx, True).start()
@@ -478,29 +501,10 @@
     own_out.start()
     own_res.start()
 
-    own_states(k_ref, v_ref, fd_ref, bd_ref, shift_ref, spike_ref, within, kd, fown, bown)
-    for k in range(1, count):
-
-        @pl.when(place + k < count)
-        def _(k=k):
-            state_copy(0, k, place + k).start()
-
-        @pl.when(place >= k)
-        def _(k=k):
-            state_copy(1, k, place - k).start()
-
     @pl.when(middle)
     def _():
         for copy in own_copies:
             copy.start()
-        for p in range(1, PIECES):
-            send_gu(place, side, p, True, sp=o)
-        relay_gu(o, 0, grp=1 - side)
-
-    @pl.when(jnp.logical_not(middle))
-    def _():
-        for p in range(1, PIECES):
-            send_gu(place, side, p, True, sp=m)
 
     fstate[...] = jnp.zeros_like(fstate)
     bstate[...] = jnp.zeros_like(bstate)
@@ -518,35 +522,21 @@
             decay = bgot[k - 1, HEAD_V : HEAD_V + 1, :].astype(F32)
             bstate[...] = bstate[...] * decay + bgot[k - 1, :HEAD_V, :].astype(F32)
 
-    relay_ow(0)
     backward_states(k_ref, v_ref, within, bstate[...], held)
-
-    @pl.when(middle)
-    def _():
-        relay_gu(o, 1, grp=1 - side)
-
-    relay_ow(1)
     attend(q_ref, k_ref, v_ref, within, gate_ref, gain_ref, fstate[...], held, attended)
     others = (tx, td, tc)
     for n, t in enumerate(others):
         a2a(n, me, t).start()
     rows[:, ds(me * width, width)] = attended[ds(me * own, own), :]
 
-    @pl.when(middle)
-    def _():
-        relay_gu(e, 0, sp=o)
-        relay_gu(e, 1, sp=o)
-        relay_gu(o, 2, grp=1 - side)
-
-    relay_ow(2)
-
-    @pl.when(middle)
-    def _():
-        relay_gu(e, 2, sp=o)
-        relay_gu(o, 3, grp=1 - side)
-        relay_gu(e, 3, sp=o)
-
-    relay_ow(3)
+    for p in range(4):
+        relay_ow(p)
+
+        @pl.when(middle)
+        def _(p=p):
+            relay_gu(o, p, grp=1 - side)
+            relay_gu(e, p, sp=o)
+
     for t in others:
         a2a(0, t, t).wait_recv()
     for t in (tc, td):
@@ -569,8 +559,7 @@
         at = slice(n * wide, (n + 1) * wide)
         acts[0, ds(me * own, own), at] = (mid[:, at].astype(F32) * inverse * norm_ref[:, at]).astype(BF16)
 
-    def target(i):
-        return pick(i, (m, o, oe, e))
+    sources = (m, m, o, o, e, oe, e, oe)
 
     @pl.when(middle)
     def _():
@@ -593,16 +582,18 @@
             ag(1, 0, me, i, tx).start()
             ag(1, 1, me, i, tc).start()
 
+        def pass_hosted(i):
+            ag(1, 2, tx, i, tc).wait_recv()
+            ag(1, 2, tx, i, tc).start()
+
         relay_gu(oe, 0, grp=1 - side)
         relay_own(0)
         relay_gu(oe, 1, grp=1 - side)
         relay_hosted(0)
         relay_gu(oe, 2, grp=1 - side)
         relay_own(1)
-        relay_hosted(1)
-        relay_gu(oe, 3, grp=1 - side)
-
-        order = [(0, 0), (0, 1), (0, 2), (1, 0), (0, 3), (1, 1), (0, 4), (1, 2), (1, 3), (1, 4)]
+
+        order = [(0, 0), (0, 1), (0, 2), (1, 0), (1, 1), (1, 2), (0, 3), (0, 4), (1, 3), (1, 4)]
 
         def first(i, carry):
             q, j = pick(i, [a for a, _ in order]), pick(i, [b for _, b in order])
@@ -615,26 +606,27 @@
 
             @pl.when(i == 1)
             def _():
+                relay_hosted(1)
+                relay_gu(oe, 3, grp=1 - side)
+                pass_hosted(0)
                 relay_gu(oe, 4, grp=1 - side)
-
-            for n in range(2):
-
-                @pl.when(i == 2 + n)
-                def _(n=n):
-                    ag(1, 2, tx, n, tc).wait_recv()
-                    ag(1, 2, tx, n, tc).start()
+                send_gu(e, side, 4, again=True, grp=1 - side)
 
             @pl.when(i == 3)
             def _():
+                pass_hosted(1)
+                relay_dn(o, 0, grp=1 - side)
                 for t in (tc, td):
                     for n in range(2):
                         ag(1, 0, t, n, tc).wait_recv()
 
-            for n in range(2):
-
-                @pl.when(i == 5 + n)
-                def _(n=n):
-                    relay_dn(o, n, grp=1 - side)
+            @pl.when(i == 6)
+            def _():
+                relay_dn(o, 1, grp=1 - side)
+
+            @pl.when(i == 8)
+            def _():
+                relay_dn(e, 0, sp=o)
 
             @pl.when(q == 0)
             def _():
@@ -655,60 +647,85 @@
             def both(block, j):
                 return part[q, i, ds(block * own, own), :].astype(F32) + got[q, i, j].astype(F32)
 
-            @pl.when(q == 0)
-            def _():
-                xsend[i] = both(tx, 1 - chip).astype(BF16)
-                xo(i).start()
-
-            @pl.when(q == 1)
-            def _():
+            @pl.when(q * (1 - i % 2) + 1 - q > 0)
+            def _():
+                xsend[q, i] = both(tx, 1 - chip).astype(BF16)
+                xo(q, i).start()
+
+            @pl.when(q * (i % 2) > 0)
+            def _():
+                esend[i, 1] = both(tx, 1 - chip).astype(BF16)
+                eo(i, 1).start()
                 esend[i, 0] = both(me, chip).astype(BF16)
                 eo(i, 0).start()
-                esend[i, 1] = both(tx, 1 - chip).astype(BF16)
-                eo(i, 1).start()
+
+        def push(i):
+            xo(1, i).wait_recv()
+            mixed = part[1, i, ds(me * own, own), :].astype(F32) + got[1, i, chip].astype(F32)
+            esend[i, 0] = (mixed + xgot[1, i].astype(F32)).astype(BF16)
+            eo(i, 0).start()
 
         def second(s, carry):
-            i, q = s // 2, s % 2
-
-            @pl.when(s == 2)
-            def _():
-                relay_dn(e, 0, sp=o)
-                for p in range(2):
-                    dn(o, 1 - side, p).wait_recv()
-
-            @pl.when(s == 3)
+            i, q = s // 2, 1 - s % 2
+
+            @pl.when((s == 6) | (s == 8) | (s == 10) | (s == 12) | (s == 14))
+            def _():
+                fold(i - 1, 0)
+
+            @pl.when(s == 4)
+            def _():
+                take_dn(o, 1 - side, 0)
+
+            @pl.when(s == 6)
             def _():
                 relay_dn(e, 1, sp=o)
+                take_dn(o, 1 - side, 1)
+
+            @pl.when(s == 8)
+            def _():
                 relay_dn(oe, 0, grp=1 - side)
-
-            @pl.when(s == 4)
+                take_dn(e, 1 - side, 0)
+
+            @pl.when(s == 10)
             def _():
                 relay_dn(oe, 1, grp=1 - side)
-                for p in range(2):
-                    dn(oe, 1 - side, p).wait_recv()
-
-            @pl.when(s == 6)
-            def _():
-                for p in range(2):
-                    dn(e, 1 - side, p).wait_recv()
-
-            part[q, i] = jnp.dot(hid[q], wd[target(i)], preferred_element_type=F32).astype(BF16)
+                take_dn(oe, 1 - side, 0)
+
+            @pl.when(s == 12)
+            def _():
+                take_dn(e, 1 - side, 1)
+
+            @pl.when(s == 14)
+            def _():
+                take_dn(oe, 1 - side, 1)
+
+            weight = wd[pick(i, sources), pick(i, (0, 1, 0, 1, 0, 0, 1, 1))]
+            part[q, i] = jnp.dot(hid[q], weight, preferred_element_type=F32).astype(BF16)
             for j in range(2):
                 cr(q, i, j).start()
 
-            @pl.when(s > 0)
-            def _():
-                fold((s - 1) // 2, (s + 1) % 2)
+            @pl.when(q == 0)
+            def _():
+                fold(i, 1)
+
+            @pl.when((s == 2) | (s == 4))
+            def _():
+                fold(i - 1, 0)
+
+            @pl.when((s == 5) | (s == 9) | (s == 13))
+            def _():
+                push(i - 2)
 
             return carry
 
-        lax.fori_loop(0, 2 * count, second, 0)
-        fold(count - 1, 1)
-
-        for i in range(count):
-            xo(i).wait_recv()
-            at = ds(target(i) * dw, dw)
-            total = part[0, i, ds(me * own, own), :].astype(F32) + got[0, i, chip].astype(F32) + xgot[i].astype(F32)
+        lax.fori_loop(0, 2 * chunks, second, 0)
+        fold(chunks - 1, 0)
+        push(chunks - 2)
+
+        for i in range(chunks):
+            xo(0, i).wait_recv()
+            at = ds((2 * sources[i] + (0, 1, 0, 1, 0, 0, 1, 1)[i]) * dw, dw)
+            total = part[0, i, ds(me * own, own), :].astype(F32) + got[0, i, chip].astype(F32) + xgot[0, i].astype(F32)
             out_ref[:, at] = (mid[:, at].astype(F32) + 0.5 * total).astype(BF16)
 
         for p in range(PIECES):
@@ -716,6 +733,8 @@
                 gu(n, place, side, p, True).wait_send()
                 for source in (e, o, oe):
                     gu(n, source, side, p).wait_send()
+        for n in range(2):
+            gu(n, e, side, 4, again=True).wait_send()
         for p in range(2):
             dn(place, side, p, True).wait_send()
             for source in (e, o, oe):
@@ -724,41 +743,53 @@
             for kind in range(3):
                 for i in range(2):
                     ag(q, kind, me, i, tc).wait_send()
-            for i in range(count):
+            for i in range(chunks):
                 for j in range(2):
                     cr(q, i, j).wait_send()
-        for i in range(count):
-            xo(i).wait_send()
-            for n in range(2):
-                eo(i, n).wait_send()
-
-    @pl.when(jnp.logical_not(middle))
+        for i in range(chunks):
+            xo(0, i).wait_send()
+            eo(i, 0).wait_send()
+            (eo(i, 1) if i % 2 else xo(1, i)).wait_send()
+
+    @pl.when(outer)
     def _():
         for i in range(2):
             to_host(i).start()
-        for p in range(PIECES):
+        for p in range(1, PIECES - 1):
             send_gu(place, 1 - side, p, True, sp=m)
         for half in (side, 1 - side):
             for p in range(2):
                 dn(place, half, p, True, sp=m).start()
-        for i in range(count):
+
+        def finish(i):
+            eo(i, 0).wait_recv()
+            total = egot[0, i].astype(F32)
+            if i % 2:
+                er(i).wait_recv()
+                total += egot[1, i].astype(F32)
+            at = ds((2 * sources[i] + (0, 1, 0, 1, 0, 0, 1, 1)[i]) * dw, dw)
+            out_ref[:, at] = (mid[:, at].astype(F32) + 0.5 * total).astype(BF16)
+
+        for i in range(1, chunks, 2):
             eo(i, 1).wait_recv()
             er(i).start()
-        for i in range(count):
-            eo(i, 0).wait_recv()
-            er(i).wait_recv()
-            at = ds(target(i) * dw, dw)
-            total = egot[0, i].astype(F32) + egot[1, i].astype(F32)
-            out_ref[:, at] = (mid[:, at].astype(F32) + 0.5 * total).astype(BF16)
+            if i > 1:
+                finish(i - 2)
+                finish(i - 3)
+        finish(chunks - 1)
+        finish(chunks - 2)
         for i in range(2):
             to_host(i).wait_send()
         for half in (side, 1 - side):
             for p in range(PIECES):
                 for n in range(2):
-                    gu(n, place, half, p, True).wait_send()
+                    if p < PIECES - 1:
+                        gu(n, place, half, p, True).wait_send()
             for p in range(2):
                 dn(place, half, p, True).wait_send()
-        for i in range(count):
+        for n in range(2):
+            gu(n, place, side, PIECES - 1, True).wait_send()
+        for i in range(1, chunks, 2):
             er(i).wait_send()
 
     for k in range(1, count):
@@ -800,7 +831,8 @@
     width = values.shape[1]
     own, model = residual.shape
     depth, hidden = gate_projection.shape
-    dw = down_projection.shape[1]
+    dw = down_projection.shape[1] // 2
+    chunks = 2 * count
     tps = tokens // own
     blocks = tokens // BLOCK
     dma = lambda *shape: pltpu.SemaphoreType.DMA(shape)
@@ -824,16 +856,16 @@
         V((2, tokens, model), BF16),
         V((PIECES, model, hidden // PIECES), BF16),
         V((PIECES, model, hidden // PIECES), BF16),
-        V((count, hidden, dw), BF16),
+        V((count, 2, hidden, dw), BF16),
         V((2, tokens, hidden), BF16),
-        V((2, count, tokens, dw), BF16),
-        V((2, count, 2, own, dw), BF16),
-        V((count, own, dw), BF16),
-        V((count, own, dw), BF16),
-        V((count, 2, own, dw), BF16),
-        V((2, count, own, dw), BF16),
-        V((count, own, dw), BF16),
-        dma(2 * PIECES + 3),
+        V((2, chunks, tokens, dw), BF16),
+        V((2, chunks, 2, own, dw), BF16),
+        V((2, chunks, own, dw), BF16),
+        V((2, chunks, own, dw), BF16),
+        V((chunks, 2, own, dw), BF16),
+        V((2, chunks, own, dw), BF16),
+        V((chunks, own, dw), BF16),
+        dma(2 * PIECES + 4),
         dma(2, count - 1),
         dma(2, count - 1),
         dma(3),
@@ -847,14 +879,14 @@
         dma(2, count, 2, PIECES),
         dma(count, 2, 2),
         dma(count, 2, 2),
-        dma(2, count, 2),
-        dma(2, count, 2),
-        dma(count),
-        dma(count),
-        dma(count, 2),
-        dma(count, 2),
-        dma(count),
-        dma(count),
+        dma(2, chunks, 2),
+        dma(2, chunks, 2),
+        dma(2, chunks),
+        dma(2, chunks),
+        dma(chunks, 2),
+        dma(chunks, 2),
+        dma(chunks),
+        dma(chunks),
     ]
     anywhere = pl.BlockSpec(memory_space=pl.ANY)
     return pl.pallas_call(
@@ -874,7 +906,7 @@
         forward_decay_logits,
         backward_decay_logits,
         decay_logit_shift,
-        jnp.transpose(decay_spike_values),
+        decay_spike_values,
         queries,
         output_gate_preact,
         head_norm_gain[None, :],

time: 160 us -> 134 us (0.84)
  Pallas kernels: 156 us -> 131 us
  local copies, waits for them, and re-layouts: 3.71 us -> 2.09 us
    pallas_call x1, Pallas kernels: 156 us -> 131 us  [fast_body(): pl.pallas_call(layer_kernel, out_shape=jax.ShapeDtypeStruct((own, model),...]
    unnamed x2 -> x1, local copies, waits for them, and re-layouts: 3.71 us -> 2.09 us
where the time goes in v1:
time: 134 us; the launch traced here: 133 us
  Pallas kernels  131 us (98%)
  local copies, waits for them, and re-layouts  2.09 us (2%)
    pallas_call x1, Pallas kernels, fast_body(): pl.pallas_call(layer_kernel, out_shape=jax.ShapeDtypeStruct((own, model),...  131 us

profile of v1, /device:TPU:0, one launch (start us, length us, event | category | flops | bytes accessed | tf_op | source)
XLA Modules:
  0.0 133.4 jit_solution(13373507134613780902)
XLA Ops:
  0.0 131.3 %layer.1 = bf16[192,2048]{1,0:T(8,128)(2,1)} custom-call(bf16[768,128]{1,0:T(8,128)(2,1)} %k_ref.1, bf16[768,256]{1,0:T(8,128)(2,1)} %v_ref.1, bf16[768,128]{1,0:T(8,128)(2,1)} %fd_ref.1, bf16[768,128]{1,0:T(8,128)(2,1)} %bd_ref.1, f32[2,128]{1,0:T(2,128)} %shift_ref.1, f32[2,768]{1,0:T(2,128)} %spike_ref.1, bf16[768,128]{1,0:T(8,128)(2,1)} %q_ref.1, ...), custom_call_target="tpu_custom_call" | custom-call | flops 30000001024 | bytes 30000000 | tf_op jit(solution)/shard_map/layer/pallas_call | solution.py:892
  131.3 2.1 %copy.17 = bf16[192,2048]{1,0:T(8,128)(2,1)} copy(bf16[192,2048]{1,0:T(8,128)(2,1)} %layer.1) | data formatting | bytes 1572864

commit v2 on v1

--- a/solution.py
+++ b/solution.py
@@ -349,8 +349,8 @@
     res_hbm, out_hbm, g_hbm, u_hbm, d_hbm,
     out_ref,
     within, kd, fown, bown, fgot, bgot, fstate, bstate, held, attended, rows, outw, res, mid, acts,
-    wg, wu, wd, hid, part, got, xsend, xgot, esend, egot, erelay,
-    loc, st_s, st_r, a2a_s, a2a_r, ow_s, ow_r, ag_s, ag_r, ea_s, gs, gr, dsd, drv, cr_s, cr_r, xo_s, xo_r,
+    wgu, wd, hid, part, got, xsend, xgot, esend, egot, erelay,
+    loc, st_s, st_r, a2a_s, a2a_r, ow_s, ow_r, ag_s, ag_r, ea_s, ea_r, gs, gr, dsd, drv, cr_s, cr_r, xo_s, xo_r,
     eo_s, eo_r, er_s, er_r,
 ):
     count = lax.axis_size("sp")
@@ -379,15 +379,15 @@
         )
 
     def gu(n, source, half, p, local=False, again=False, **dev):
-        dst = (wg, wu)[n].at[p, ds(source * depth + half * hr, hr), :]
+        dst = wgu.at[n, p, ds(source * depth + half * hr, hr), :]
         src = (g_hbm, u_hbm)[n].at[ds(half * hr, hr), ds(p * tile, tile)] if local else dst
-        send = gs.at[n, source, 1 - half if again else half, p]
+        send = gs.at[source, 1 - half if again else half]
         return remote(src, dst, send, gr.at[n, source, half, p], **(dev or dict(sp=o)))
 
-    def dn(source, half, p, local=False, **dev):
-        dst = wd.at[source, p, ds(half * dr, dr), :]
-        src = d_hbm.at[ds(half * dr, dr), p * dw : (p + 1) * dw] if local else dst
-        return remote(src, dst, dsd.at[source, half, p], drv.at[source, half, p], **(dev or dict(sp=o)))
+    def dn(source, half, p, r, local=False, **dev):
+        dst = wd.at[source, p, ds(half * dr + r * (dr // 2), dr // 2), :]
+        src = d_hbm.at[ds(half * dr + r * (dr // 2), dr // 2), p * dw : (p + 1) * dw] if local else dst
+        return remote(src, dst, dsd.at[source, half], drv.at[source, half, p, r], **(dev or dict(sp=o)))
 
     def send_gu(source, half, p, local=False, again=False, **dev):
         for n in range(2):
@@ -398,23 +398,42 @@
             gu(n, source, half, p).wait_recv()
 
     def relay_gu(source, p, **dev):
-        take_gu(source, side, p)
-        send_gu(source, side, p, **dev)
+        for n in range(2):
+            gu(n, source, side, p).wait_recv()
+            gu(n, source, side, p, **dev).start()
+
+    def send_dn(half, p, **dev):
+        for r in range(2):
+            dn(place, half, p, r, True, **dev).start()
 
     def take_dn(source, half, p):
-        dn(source, half, p).wait_recv()
-
-    def relay_dn(source, p, **dev):
-        take_dn(source, side, p)
-        dn(source, side, p, **dev).start()
+        for r in range(2):
+            dn(source, half, p, r).wait_recv()
+
+    def relay_dn(source, p, r, **dev):
+        dn(source, side, p, r).wait_recv()
+        dn(source, side, p, r, **dev).start()
+
+    def sent(ref, sem):
+        remote(ref, ref, sem, sem, sp=o).wait_send()
+
+    def sent_gu(source, half, low, high, again=False):
+        at = ds(source * depth + half * hr, hr)
+        sent(wgu.at[:, low:high, at, :], gs.at[source, 1 - half if again else half])
+
+    def sent_dn(source, half, low, high):
+        sent(wd.at[source, low:high, ds(half * dr, dr), :], dsd.at[source, half])
+
+    def landed(ref, sem):
+        remote(ref, ref, sem, sem, sp=o).wait_recv()
 
     def ow(kind, block, i, dev, local=False):
         dst = outw.at[ds(block * width + i * orow, orow), :]
         src = out_hbm.at[i * orow : (i + 1) * orow, :] if local else dst
-        return remote(src, dst, ow_s.at[kind, i], ow_r.at[block, i], tp=dev)
+        return remote(src, dst, ow_s.at[kind], ow_r.at[i if kind == 0 else 3 + kind], tp=dev)
 
     def relay_ow(i):
-        ow(2, tx, i, tc).wait_recv()
+        ow(0, tx, i, tc).wait_recv()
         ow(2, tx, i, tc).start()
 
     def a2a(n, block, dev):
@@ -424,11 +443,15 @@
 
     def ag(q, kind, block, i, dev):
         at = acts.at[q, ds(block * own + i * nrow, nrow), :]
-        return remote(at, at, ag_s.at[q, kind, i], ag_r.at[q, block, i], tp=dev)
+        return remote(at, at, ag_s.at[q, kind], ag_r.at[q, i if kind == 0 else 1 + kind], tp=dev)
 
     def to_host(i):
         at = ds(me * own + i * nrow, nrow)
-        return remote(acts.at[0, at, :], acts.at[1, at, :], ea_s.at[i], ag_r.at[1, me, i], sp=m)
+        return remote(acts.at[0, at, :], acts.at[1, at, :], ea_s.at[0], ea_r.at[i], sp=m)
+
+    def gathered(q):
+        for kind, block in ((1, tc), (2, td)):
+            landed(acts.at[q, ds(block * own, own), :], ag_r.at[q, 1 + kind])
 
     def state_copy(n, k, dev):
         src, dst = ((fown, fgot), (bown, bgot))[n]
@@ -436,17 +459,17 @@
 
     def cr(q, i, j):
         block = 2 * j + 1 - core
-        return remote(part.at[q, i, ds(block * own, own), :], got.at[q, i, j], cr_s.at[q, i, j], cr_r.at[q, i, j], tp=tc)
+        return remote(part.at[q, i, ds(block * own, own), :], got.at[q, i, j], cr_s.at[q], cr_r.at[q, i], tp=tc)
 
     def xo(q, i):
-        return remote(xsend.at[q, i], xgot.at[q, i], xo_s.at[q, i], xo_r.at[q, i], tp=tx)
+        return remote(xsend.at[q, i], xgot.at[q, i], xo_s.at[q], xo_r.at[q, i], tp=tx)
 
     def eo(i, n):
         dst = egot.at[0, i] if n == 0 else erelay.at[i]
-        return remote(esend.at[i, n], dst, eo_s.at[i, n], eo_r.at[i, n], sp=e)
+        return remote(esend.at[i, n], dst, eo_s.at[n], eo_r.at[i, n], sp=e)
 
     def er(i):
-        return remote(erelay.at[i], egot.at[1, i], er_s.at[i], er_r.at[i], tp=tx)
+        return remote(erelay.at[i], egot.at[1, i], er_s.at[0], er_r.at[i], tp=tx)
 
     own_copies = []
     for p in range(PIECES):
@@ -454,16 +477,19 @@
             own_copies.append(
                 pltpu.make_async_copy(
                     (g_hbm, u_hbm)[n].at[:, p * tile : (p + 1) * tile],
-                    (wg, wu)[n].at[p, ds(place * depth, depth), :],
-                    loc.at[n * PIECES + p],
+                    wgu.at[n, p, ds(place * depth, depth), :],
+                    loc.at[0],
                 )
             )
     for p in range(2):
-        own_copies.append(
-            pltpu.make_async_copy(d_hbm.at[:, p * dw : (p + 1) * dw], wd.at[place, p], loc.at[2 * PIECES + p])
-        )
-    own_out = pltpu.make_async_copy(out_hbm, outw.at[ds(me * width, width), :], loc.at[2 * PIECES + 2])
-    own_res = pltpu.make_async_copy(res_hbm, res, loc.at[2 * PIECES + 3])
+        own_copies.append(pltpu.make_async_copy(d_hbm.at[:, p * dw : (p + 1) * dw], wd.at[place, p], loc.at[1]))
+    own_gu = wgu.at[:, :, ds(place * depth, depth), :]
+    own_waits = [
+        pltpu.make_async_copy(own_gu, own_gu, loc.at[0]),
+        pltpu.make_async_copy(wd.at[place], wd.at[place], loc.at[1]),
+    ]
+    own_out = pltpu.make_async_copy(out_hbm, outw.at[ds(me * width, width), :], loc.at[2])
+    own_res = pltpu.make_async_copy(res_hbm, res, loc.at[3])
 
     barrier = pltpu.get_barrier_semaphore()
     friends = [dict(sp=lax.rem(place + k, count)) for k in range(1, count)]
@@ -539,9 +565,8 @@
 
     for t in others:
         a2a(0, t, t).wait_recv()
-    for t in (tc, td):
-        for i in range(4):
-            ow(0, t, i, tc).wait_recv()
+    for kind, t in ((1, tc), (2, td)):
+        landed(outw.at[ds(t * width, width), :], ow_r.at[3 + kind])
     own_out.wait()
     own_res.wait()
 
@@ -559,7 +584,8 @@
         at = slice(n * wide, (n + 1) * wide)
         acts[0, ds(me * own, own), at] = (mid[:, at].astype(F32) * inverse * norm_ref[:, at]).astype(BF16)
 
-    sources = (m, m, o, o, e, oe, e, oe)
+    sources = (m, m, o, oe, e, o, oe, e)
+    sides = (0, 1, 0, 0, 0, 1, 1, 1)
 
     @pl.when(middle)
     def _():
@@ -569,21 +595,21 @@
         relay_gu(o, 4, grp=1 - side)
         relay_gu(e, 4, sp=o)
         for p in range(2):
-            dn(place, side, p, True, sp=o).start()
-        for copy in own_copies:
+            send_dn(side, p, sp=o)
+        for copy in own_waits:
             copy.wait()
 
         def relay_own(i):
-            ag(0, 2, tx, i, tc).wait_recv()
+            ag(0, 0, tx, i, tc).wait_recv()
             ag(0, 2, tx, i, tc).start()
 
         def relay_hosted(i):
-            ag(1, 0, me, i, tx).wait_recv()
+            to_host(i).wait_recv()
             ag(1, 0, me, i, tx).start()
             ag(1, 1, me, i, tc).start()
 
         def pass_hosted(i):
-            ag(1, 2, tx, i, tc).wait_recv()
+            ag(1, 0, tx, i, tc).wait_recv()
             ag(1, 2, tx, i, tc).start()
 
         relay_gu(oe, 0, grp=1 - side)
@@ -600,49 +626,45 @@
 
             @pl.when(i == 0)
             def _():
-                for t in (tc, td):
-                    for n in range(2):
-                        ag(0, 0, t, n, tc).wait_recv()
+                gathered(0)
 
             @pl.when(i == 1)
             def _():
                 relay_hosted(1)
                 relay_gu(oe, 3, grp=1 - side)
                 pass_hosted(0)
+
+            @pl.when(i == 2)
+            def _():
                 relay_gu(oe, 4, grp=1 - side)
                 send_gu(e, side, 4, again=True, grp=1 - side)
+                pass_hosted(1)
 
             @pl.when(i == 3)
             def _():
-                pass_hosted(1)
-                relay_dn(o, 0, grp=1 - side)
-                for t in (tc, td):
-                    for n in range(2):
-                        ag(1, 0, t, n, tc).wait_recv()
-
-            @pl.when(i == 6)
-            def _():
-                relay_dn(o, 1, grp=1 - side)
+                for r in range(2):
+                    relay_dn(o, 0, r, grp=1 - side)
+                gathered(1)
 
             @pl.when(i == 8)
             def _():
-                relay_dn(e, 0, sp=o)
+                for r in range(2):
+                    relay_dn(e, 0, r, sp=o)
 
             @pl.when(q == 0)
             def _():
                 for source in (o, oe, e):
                     take_gu(source, 1 - side, j)
 
-            g = jnp.dot(acts[q], wg[j], preferred_element_type=F32)
-            u = jnp.dot(acts[q], wu[j], preferred_element_type=F32)
+            g = jnp.dot(acts[q], wgu[0, j], preferred_element_type=F32)
+            u = jnp.dot(acts[q], wgu[1, j], preferred_element_type=F32)
             hid[q, :, ds(j * tile, tile)] = (g * jax.nn.sigmoid(g) * u).astype(BF16)
             return carry
 
         lax.fori_loop(0, len(order), first, 0)
 
         def fold(i, q):
-            for j in range(2):
-                cr(q, i, j).wait_recv()
+            landed(got.at[q, i], cr_r.at[q, i])
 
             def both(block, j):
                 return part[q, i, ds(block * own, own), :].astype(F32) + got[q, i, j].astype(F32)
@@ -672,34 +694,42 @@
             def _():
                 fold(i - 1, 0)
 
+            @pl.when(s == 2)
+            def _():
+                relay_dn(e, 1, 0, sp=o)
+
             @pl.when(s == 4)
             def _():
+                relay_dn(oe, 0, 0, grp=1 - side)
+                relay_dn(e, 1, 1, sp=o)
+                send_dn(1 - side, 1, sp=o)
                 take_dn(o, 1 - side, 0)
 
             @pl.when(s == 6)
             def _():
-                relay_dn(e, 1, sp=o)
+                relay_dn(oe, 0, 1, grp=1 - side)
+                relay_dn(oe, 1, 0, grp=1 - side)
+                take_dn(oe, 1 - side, 0)
+
+            @pl.when(s == 8)
+            def _():
+                relay_dn(oe, 1, 1, grp=1 - side)
+                take_dn(e, 1 - side, 0)
+
+            @pl.when(s == 10)
+            def _():
+                take_dn(o, side, 1)
                 take_dn(o, 1 - side, 1)
 
-            @pl.when(s == 8)
-            def _():
-                relay_dn(oe, 0, grp=1 - side)
-                take_dn(e, 1 - side, 0)
-
-            @pl.when(s == 10)
-            def _():
-                relay_dn(oe, 1, grp=1 - side)
-                take_dn(oe, 1 - side, 0)
-
             @pl.when(s == 12)
             def _():
+                take_dn(oe, 1 - side, 1)
+
+            @pl.when(s == 14)
+            def _():
                 take_dn(e, 1 - side, 1)
 
-            @pl.when(s == 14)
-            def _():
-                take_dn(oe, 1 - side, 1)
-
-            weight = wd[pick(i, sources), pick(i, (0, 1, 0, 1, 0, 0, 1, 1))]
+            weight = wd[pick(i, sources), pick(i, sides)]
             part[q, i] = jnp.dot(hid[q], weight, preferred_element_type=F32).astype(BF16)
             for j in range(2):
                 cr(q, i, j).start()
@@ -724,32 +754,25 @@
 
         for i in range(chunks):
             xo(0, i).wait_recv()
-            at = ds((2 * sources[i] + (0, 1, 0, 1, 0, 0, 1, 1)[i]) * dw, dw)
+            at = ds((2 * sources[i] + sides[i]) * dw, dw)
             total = part[0, i, ds(me * own, own), :].astype(F32) + got[0, i, chip].astype(F32) + xgot[0, i].astype(F32)
             out_ref[:, at] = (mid[:, at].astype(F32) + 0.5 * total).astype(BF16)
 
-        for p in range(PIECES):
-            for n in range(2):
-                gu(n, place, side, p, True).wait_send()
-                for source in (e, o, oe):
-                    gu(n, source, side, p).wait_send()
-        for n in range(2):
-            gu(n, e, side, 4, again=True).wait_send()
-        for p in range(2):
-            dn(place, side, p, True).wait_send()
-            for source in (e, o, oe):
-                dn(source, side, p).wait_send()
+        for source in (place, e, o, oe):
+            sent_gu(source, side, 0, PIECES)
+        sent_gu(e, side, 4, 5, again=True)
+        for source in (place, e, oe):
+            sent_dn(source, side, 0, 2)
+        sent_dn(o, side, 0, 1)
+        sent_dn(place, 1 - side, 1, 2)
         for q in range(2):
             for kind in range(3):
-                for i in range(2):
-                    ag(q, kind, me, i, tc).wait_send()
-            for i in range(chunks):
-                for j in range(2):
-                    cr(q, i, j).wait_send()
-        for i in range(chunks):
-            xo(0, i).wait_send()
-            eo(i, 0).wait_send()
-            (eo(i, 1) if i % 2 else xo(1, i)).wait_send()
+                sent(acts.at[q, ds(me * own, own), :], ag_s.at[q, kind])
+            sent(got.at[q], cr_s.at[q])
+        sent(xsend.at[0], xo_s.at[0])
+        sent(xsend.at[1, : chunks // 2], xo_s.at[1])
+        sent(esend.at[:, 0], eo_s.at[0])
+        sent(esend.at[: chunks // 2, 1], eo_s.at[1])
 
     @pl.when(outer)
     def _():
@@ -759,7 +782,7 @@
             send_gu(place, 1 - side, p, True, sp=m)
         for half in (side, 1 - side):
             for p in range(2):
-                dn(place, half, p, True, sp=m).start()
+                send_dn(half, p, sp=m)
 
         def finish(i):
             eo(i, 0).wait_recv()
@@ -767,7 +790,7 @@
             if i % 2:
                 er(i).wait_recv()
                 total += egot[1, i].astype(F32)
-            at = ds((2 * sources[i] + (0, 1, 0, 1, 0, 0, 1, 1)[i]) * dw, dw)
+            at = ds((2 * sources[i] + sides[i]) * dw, dw)
             out_ref[:, at] = (mid[:, at].astype(F32) + 0.5 * total).astype(BF16)
 
         for i in range(1, chunks, 2):
@@ -778,19 +801,12 @@
                 finish(i - 3)
         finish(chunks - 1)
         finish(chunks - 2)
-        for i in range(2):
-            to_host(i).wait_send()
+        sent(acts.at[0, ds(me * own, own), :], ea_s.at[0])
+        sent_gu(place, side, 0, PIECES)
+        sent_gu(place, 1 - side, 0, PIECES - 1)
         for half in (side, 1 - side):
-            for p in range(PIECES):
-                for n in range(2):
-                    if p < PIECES - 1:
-                        gu(n, place, half, p, True).wait_send()
-            for p in range(2):
-                dn(place, half, p, True).wait_send()
-        for n in range(2):
-            gu(n, place, side, PIECES - 1, True).wait_send()
-        for i in range(1, chunks, 2):
-            er(i).wait_send()
+            sent_dn(place, half, 0, 2)
+        sent(erelay.at[: chunks // 2], er_s.at[0])
 
     for k in range(1, count):
 
@@ -805,8 +821,7 @@
     for n, t in enumerate(others):
         a2a(n, me, t).wait_send()
     for kind in range(3):
-        for i in range(4):
-            ow(kind, me, i, tc).wait_send()
+        sent(outw.at[ds(me * width, width), :], ow_s.at[kind])
 
 
 def fast_body(
@@ -854,8 +869,7 @@
         V((own, model), BF16),
         V((own, model), BF16),
         V((2, tokens, model), BF16),
-        V((PIECES, model, hidden // PIECES), BF16),
-        V((PIECES, model, hidden // PIECES), BF16),
+        V((2, PIECES, model, hidden // PIECES), BF16),
         V((count, 2, hidden, dw), BF16),
         V((2, tokens, hidden), BF16),
         V((2, chunks, tokens, dw), BF16),
@@ -865,27 +879,28 @@
         V((chunks, 2, own, dw), BF16),
         V((2, chunks, own, dw), BF16),
         V((chunks, own, dw), BF16),
-        dma(2 * PIECES + 4),
+        dma(4),
         dma(2, count - 1),
         dma(2, count - 1),
         dma(3),
         dma(tps),
-        dma(3, 4),
-        dma(tps, 4),
-        dma(2, 3, 2),
-        dma(2, tps, 2),
+        dma(3),
+        dma(6),
+        dma(2, 3),
+        dma(2, 4),
+        dma(1),
         dma(2),
+        dma(count, 2),
         dma(2, count, 2, PIECES),
-        dma(2, count, 2, PIECES),
-        dma(count, 2, 2),
-        dma(count, 2, 2),
-        dma(2, chunks, 2),
-        dma(2, chunks, 2),
+        dma(count, 2),
+        dma(count, 2, 2, 2),
+        dma(2),
         dma(2, chunks),
+        dma(2),
         dma(2, chunks),
+        dma(2),
         dma(chunks, 2),
-        dma(chunks, 2),
-        dma(chunks),
+        dma(1),
         dma(chunks),
     ]
     anywhere = pl.BlockSpec(memory_space=pl.ANY)

time: 134 us -> 132 us (0.985)
    pallas_call x1, Pallas kernels: 131 us -> 130 us  [fast_body(): pl.pallas_call(layer_kernel, out_shape=jax.ShapeDtypeStruct((own, model),...]
where the time goes in v2:
time: 132 us
  Pallas kernels  130 us (98%)
  local copies, waits for them, and re-layouts  2.09 us (2%)
    pallas_call x1, Pallas kernels, fast_body(): pl.pallas_call(layer_kernel, out_shape=jax.ShapeDtypeStruct((own, model),...  130 us

profile of v2, /device:TPU:0, one launch (start us, length us, event | category | flops | bytes accessed | tf_op | source)
XLA Modules:
  0.0 131.8 jit_solution(16986375334257358071)
XLA Ops:
  0.0 129.7 %layer.1 = bf16[192,2048]{1,0:T(8,128)(2,1)} custom-call(bf16[768,128]{1,0:T(8,128)(2,1)} %k_ref.1, bf16[768,256]{1,0:T(8,128)(2,1)} %v_ref.1, bf16[768,128]{1,0:T(8,128)(2,1)} %fd_ref.1, bf16[768,128]{1,0:T(8,128)(2,1)} %bd_ref.1, f32[2,128]{1,0:T(2,128)} %shift_ref.1, f32[2,768]{1,0:T(2,128)} %spike_ref.1, bf16[768,128]{1,0:T(8,128)(2,1)} %q_ref.1, ...), custom_call_target="tpu_custom_call" | custom-call | flops 30000001024 | bytes 30000000 | tf_op jit(solution)/shard_map/layer/pallas_call | solution.py:907
  129.7 2.1 %copy.17 = bf16[192,2048]{1,0:T(8,128)(2,1)} copy(bf16[192,2048]{1,0:T(8,128)(2,1)} %layer.1) | data formatting | bytes 1572864

commit v3 on v2

--- a/solution.py
+++ b/solution.py
@@ -345,9 +345,10 @@
 
 
 def layer_kernel(
-    k_ref, v_ref, fd_ref, bd_ref, shift_ref, spike_ref, q_ref, gate_ref, gain_ref, norm_ref,
+    k_hbm, v_hbm, fd_hbm, bd_hbm, shift_hbm, spike_hbm, q_hbm, gate_hbm, gain_hbm, norm_hbm,
     res_hbm, out_hbm, g_hbm, u_hbm, d_hbm,
     out_ref,
+    k_ref, v_ref, fd_ref, bd_ref, shift_ref, spike_ref, q_ref, gate_ref, gain_ref, norm_ref, in_s,
     within, kd, fown, bown, fgot, bgot, fstate, bstate, held, attended, rows, outw, res, mid, acts,
     wgu, wd, hid, part, got, xsend, xgot, esend, egot, erelay,
     loc, st_s, st_r, a2a_s, a2a_r, ow_s, ow_r, ag_s, ag_r, ea_s, ea_r, gs, gr, dsd, drv, cr_s, cr_r, xo_s, xo_r,
@@ -496,34 +497,66 @@
     friends += [dict(grp=1 - side)] + [dict(tp=t) for t in (tc, tx, td)]
     for friend in friends:
         pl.semaphore_signal(barrier, inc=1, device_id=friend, device_id_type=MESH)
-    own_states(k_ref, v_ref, fd_ref, bd_ref, shift_ref, spike_ref, within, kd, fown, bown)
+    loads = [
+        pltpu.make_async_copy(src, dst, in_s.at[n])
+        for n, (src, dst) in enumerate(
+            (
+                (k_hbm, k_ref),
+                (v_hbm, v_ref),
+                (fd_hbm, fd_ref),
+                (bd_hbm, bd_ref),
+                (shift_hbm, shift_ref),
+                (spike_hbm, spike_ref),
+                (q_hbm, q_ref),
+                (gate_hbm, gate_ref),
+                (gain_hbm, gain_ref),
+                (norm_hbm, norm_ref),
+            )
+        )
+    ]
+    for load in loads:
+        load.start()
     pl.semaphore_wait(barrier, len(friends))
-
-    for k in range(1, count):
-
-        @pl.when(place + k < count)
-        def _(k=k):
-            state_copy(0, k, place + k).start()
-
-        @pl.when(place >= k)
-        def _(k=k):
-            state_copy(1, k, place - k).start()
 
     @pl.when(middle)
     def _():
-        for p in range(PIECES):
-            send_gu(place, side, p, True, sp=o)
+        gu(0, place, side, 0, True, sp=o).start()
 
     @pl.when(outer)
     def _():
-        for p in range(PIECES):
-            send_gu(place, side, p, True, sp=m)
-        send_gu(place, 1 - side, 0, True, sp=m)
+        gu(0, place, side, 0, True, sp=m).start()
 
     for i in range(4):
         ow(0, me, i, tx, True).start()
     for i in range(4):
         ow(1, me, i, tc, True).start()
+    for load in loads[:6]:
+        load.wait()
+    own_states(k_ref, v_ref, fd_ref, bd_ref, shift_ref, spike_ref, within, kd, fown, bown)
+
+    for k in range(1, count):
+
+        @pl.when(place + k < count)
+        def _(k=k):
+            state_copy(0, k, place + k).start()
+
+        @pl.when(place >= k)
+        def _(k=k):
+            state_copy(1, k, place - k).start()
+
+    @pl.when(middle)
+    def _():
+        gu(1, place, side, 0, True, sp=o).start()
+        for p in range(1, PIECES):
+            send_gu(place, side, p, True, sp=o)
+
+    @pl.when(outer)
+    def _():
+        gu(1, place, side, 0, True, sp=m).start()
+        for p in range(1, PIECES):
+            send_gu(place, side, p, True, sp=m)
+        send_gu(place, 1 - side, 0, True, sp=m)
+
     own_out.start()
     own_res.start()
 
@@ -532,6 +565,8 @@
         for copy in own_copies:
             copy.start()
 
+    for load in loads[6:]:
+        load.wait()
     fstate[...] = jnp.zeros_like(fstate)
     bstate[...] = jnp.zeros_like(bstate)
     for k in reversed(range(1, count)):
@@ -584,7 +619,7 @@
         at = slice(n * wide, (n + 1) * wide)
         acts[0, ds(me * own, own), at] = (mid[:, at].astype(F32) * inverse * norm_ref[:, at]).astype(BF16)
 
-    sources = (m, m, o, oe, e, o, oe, e)
+    sources = (m, m, o, e, oe, e, oe, o)
     sides = (0, 1, 0, 0, 0, 1, 1, 1)
 
     @pl.when(middle)
@@ -594,6 +629,8 @@
             ag(0, 1, me, i, tc).start()
         relay_gu(o, 4, grp=1 - side)
         relay_gu(e, 4, sp=o)
+        for p in (4, 3):
+            send_gu(e, side, p, again=True, grp=1 - side)
         for p in range(2):
             send_dn(side, p, sp=o)
         for copy in own_waits:
@@ -637,19 +674,31 @@
             @pl.when(i == 2)
             def _():
                 relay_gu(oe, 4, grp=1 - side)
-                send_gu(e, side, 4, again=True, grp=1 - side)
+
+            @pl.when(i == 3)
+            def _():
                 pass_hosted(1)
-
-            @pl.when(i == 3)
-            def _():
                 for r in range(2):
                     relay_dn(o, 0, r, grp=1 - side)
                 gathered(1)
 
+            @pl.when(i == 4)
+            def _():
+                relay_dn(e, 0, 0, sp=o)
+
+            @pl.when(i == 5)
+            def _():
+                relay_dn(e, 0, 1, sp=o)
+
+            @pl.when(i == 7)
+            def _():
+                relay_dn(e, 1, 0, sp=o)
+
             @pl.when(i == 8)
             def _():
-                for r in range(2):
-                    relay_dn(e, 0, r, sp=o)
+                relay_dn(oe, 0, 0, grp=1 - side)
+                relay_dn(e, 1, 1, sp=o)
+                send_dn(1 - side, 1, sp=o)
 
             @pl.when(q == 0)
             def _():
@@ -690,66 +739,61 @@
         def second(s, carry):
             i, q = s // 2, 1 - s % 2
 
-            @pl.when((s == 6) | (s == 8) | (s == 10) | (s == 12) | (s == 14))
-            def _():
-                fold(i - 1, 0)
-
-            @pl.when(s == 2)
-            def _():
-                relay_dn(e, 1, 0, sp=o)
+            @pl.when(s == 0)
+            def _():
+                relay_dn(oe, 0, 1, grp=1 - side)
 
             @pl.when(s == 4)
             def _():
-                relay_dn(oe, 0, 0, grp=1 - side)
-                relay_dn(e, 1, 1, sp=o)
-                send_dn(1 - side, 1, sp=o)
                 take_dn(o, 1 - side, 0)
 
+            @pl.when(s == 5)
+            def _():
+                relay_dn(oe, 1, 0, grp=1 - side)
+
             @pl.when(s == 6)
             def _():
-                relay_dn(oe, 0, 1, grp=1 - side)
-                relay_dn(oe, 1, 0, grp=1 - side)
+                take_dn(e, 1 - side, 0)
+
+            @pl.when(s == 8)
+            def _():
                 take_dn(oe, 1 - side, 0)
 
-            @pl.when(s == 8)
+            @pl.when(s == 10)
             def _():
                 relay_dn(oe, 1, 1, grp=1 - side)
-                take_dn(e, 1 - side, 0)
-
-            @pl.when(s == 10)
+                fold(4, 1)
+                fold(4, 0)
+                push(2)
+                take_dn(e, 1 - side, 1)
+
+            @pl.when(s == 12)
+            def _():
+                take_dn(oe, 1 - side, 1)
+
+            @pl.when(s == 14)
             def _():
                 take_dn(o, side, 1)
                 take_dn(o, 1 - side, 1)
-
-            @pl.when(s == 12)
-            def _():
-                take_dn(oe, 1 - side, 1)
-
-            @pl.when(s == 14)
-            def _():
-                take_dn(e, 1 - side, 1)
 
             weight = wd[pick(i, sources), pick(i, sides)]
             part[q, i] = jnp.dot(hid[q], weight, preferred_element_type=F32).astype(BF16)
             for j in range(2):
                 cr(q, i, j).start()
 
-            @pl.when(q == 0)
-            def _():
-                fold(i, 1)
-
-            @pl.when((s == 2) | (s == 4))
-            def _():
-                fold(i - 1, 0)
-
-            @pl.when((s == 5) | (s == 9) | (s == 13))
-            def _():
-                push(i - 2)
+            @pl.when(((s > 1) & (s < 10)) | (s > 11))
+            def _():
+                fold(i - 1, q)
+
+            @pl.when((s == 9) | (s == 12))
+            def _():
+                push(pick(s - 9, (0, 4, 4, 4)))
 
             return carry
 
         lax.fori_loop(0, 2 * chunks, second, 0)
-        fold(chunks - 1, 0)
+        for q in (1, 0):
+            fold(chunks - 1, q)
         push(chunks - 2)
 
         for i in range(chunks):
@@ -760,7 +804,7 @@
 
         for source in (place, e, o, oe):
             sent_gu(source, side, 0, PIECES)
-        sent_gu(e, side, 4, 5, again=True)
+        sent_gu(e, side, PIECES - 2, PIECES, again=True)
         for source in (place, e, oe):
             sent_dn(source, side, 0, 2)
         sent_dn(o, side, 0, 1)
@@ -778,7 +822,7 @@
     def _():
         for i in range(2):
             to_host(i).start()
-        for p in range(1, PIECES - 1):
+        for p in range(1, PIECES - 2):
             send_gu(place, 1 - side, p, True, sp=m)
         for half in (side, 1 - side):
             for p in range(2):
@@ -803,7 +847,7 @@
         finish(chunks - 2)
         sent(acts.at[0, ds(me * own, own), :], ea_s.at[0])
         sent_gu(place, side, 0, PIECES)
-        sent_gu(place, 1 - side, 0, PIECES - 1)
+        sent_gu(place, 1 - side, 0, PIECES - 2)
         for half in (side, 1 - side):
             sent_dn(place, half, 0, 2)
         sent(erelay.at[: chunks // 2], er_s.at[0])
@@ -854,6 +898,17 @@
     state = (HEAD_V + 16, lanes)
     V = pltpu.VMEM
     scratch = [
+        V((tokens, lanes), BF16),
+        V((tokens, width), BF16),
+        V((tokens, lanes), BF16),
+        V((tokens, lanes), BF16),
+        V(decay_logit_shift.shape, F32),
+        V(decay_spike_values.shape, F32),
+        V((tokens, lanes), BF16),
+        V((tokens, width), BF16),
+        V((1, width), F32),
+        V((1, model), F32),
+        dma(10),
         V((tokens, 2 * lanes), F32),
         V((tokens, 2 * lanes), BF16),
         V(state, BF16),
@@ -906,12 +961,12 @@
     anywhere = pl.BlockSpec(memory_space=pl.ANY)
     return pl.pallas_call(
         layer_kernel,
-        out_shape=jax.ShapeDtypeStruct((own, model), BF16),
-        in_specs=[VMEM] * 10 + [anywhere] * 5,
+        out_shape=pltpu.MemorySpace.VMEM((own, model), BF16),
+        in_specs=[anywhere] * 15,
         out_specs=VMEM,
         scratch_shapes=scratch,
         compiler_params=pltpu.CompilerParams(
-            collective_id=0, has_side_effects=True, vmem_limit_bytes=67043328
+            collective_id=0, has_side_effects=True, vmem_limit_bytes=61000000
         ),
         cost_estimate=cost(3 * 10**10, 3 * 10**7),
         name="layer",

time: 132 us -> 126 us (0.955)
  Pallas kernels: 130 us -> 124 us
    pallas_call x1, Pallas kernels: 130 us -> 124 us  [fast_body(): pl.pallas_call(layer_kernel, out_shape=pltpu.MemorySpace.VMEM((own, model...]
where the time goes in v3:
time: 126 us; the launch traced here: 125 us
  Pallas kernels  124 us (98%)
    pallas_call x1, Pallas kernels, fast_body(): pl.pallas_call(layer_kernel, out_shape=pltpu.MemorySpace.VMEM((own, model...  124 us

profile of v3, /device:TPU:0, one launch (start us, length us, event | category | flops | bytes accessed | tf_op | source)
XLA Modules:
  0.0 125.4 jit_solution(12074985735002634085)
XLA Ops:
  0.0 124.5 %layer.1 = bf16[192,2048]{1,0:T(8,128)(2,1)S(1)} custom-call(bf16[768,128]{1,0:T(8,128)(2,1)} %k_hbm.1, bf16[768,256]{1,0:T(8,128)(2,1)} %v_hbm.1, bf16[768,128]{1,0:T(8,128)(2,1)} %fd_hbm.1, bf16[768,128]{1,0:T(8,128)(2,1)} %bd_hbm.1, f32[2,128]{1,0:T(2,128)} %shift_hbm.1, f32[2,768]{1,0:T(2,128)} %spike_hbm.1, bf16[768,128]{1,0:T(8,128)(2,1)} %q_hbm.1, ...), custom_call_target="tpu_custom_call" | custom-call | flops 30000001024 | bytes 30000000 | tf_op jit(solution)/shard_map/layer/pallas_call | solution.py:962
  124.5 0.9 copy.17

commit v4 on v3

--- a/solution.py
+++ b/solution.py
@@ -619,6 +619,12 @@
         at = slice(n * wide, (n + 1) * wide)
         acts[0, ds(me * own, own), at] = (mid[:, at].astype(F32) * inverse * norm_ref[:, at]).astype(BF16)
 
+    direct = (1, 1, 0, 0, 0, 1, 0, 1)
+    whole = [i for i, d in enumerate(direct) if d]
+
+    def straight(i):
+        return direct[i] if isinstance(i, int) else pick(i, direct)
+
     sources = (m, m, o, e, oe, e, oe, o)
     sides = (0, 1, 0, 0, 0, 1, 1, 1)
 
@@ -629,8 +635,7 @@
             ag(0, 1, me, i, tc).start()
         relay_gu(o, 4, grp=1 - side)
         relay_gu(e, 4, sp=o)
-        for p in (4, 3):
-            send_gu(e, side, p, again=True, grp=1 - side)
+        send_gu(e, side, PIECES - 1, again=True, grp=1 - side)
         for p in range(2):
             send_dn(side, p, sp=o)
         for copy in own_waits:
@@ -656,61 +661,7 @@
         relay_gu(oe, 2, grp=1 - side)
         relay_own(1)
 
-        order = [(0, 0), (0, 1), (0, 2), (1, 0), (1, 1), (1, 2), (0, 3), (0, 4), (1, 3), (1, 4)]
-
-        def first(i, carry):
-            q, j = pick(i, [a for a, _ in order]), pick(i, [b for _, b in order])
-
-            @pl.when(i == 0)
-            def _():
-                gathered(0)
-
-            @pl.when(i == 1)
-            def _():
-                relay_hosted(1)
-                relay_gu(oe, 3, grp=1 - side)
-                pass_hosted(0)
-
-            @pl.when(i == 2)
-            def _():
-                relay_gu(oe, 4, grp=1 - side)
-
-            @pl.when(i == 3)
-            def _():
-                pass_hosted(1)
-                for r in range(2):
-                    relay_dn(o, 0, r, grp=1 - side)
-                gathered(1)
-
-            @pl.when(i == 4)
-            def _():
-                relay_dn(e, 0, 0, sp=o)
-
-            @pl.when(i == 5)
-            def _():
-                relay_dn(e, 0, 1, sp=o)
-
-            @pl.when(i == 7)
-            def _():
-                relay_dn(e, 1, 0, sp=o)
-
-            @pl.when(i == 8)
-            def _():
-                relay_dn(oe, 0, 0, grp=1 - side)
-                relay_dn(e, 1, 1, sp=o)
-                send_dn(1 - side, 1, sp=o)
-
-            @pl.when(q == 0)
-            def _():
-                for source in (o, oe, e):
-                    take_gu(source, 1 - side, j)
-
-            g = jnp.dot(acts[q], wgu[0, j], preferred_element_type=F32)
-            u = jnp.dot(acts[q], wgu[1, j], preferred_element_type=F32)
-            hid[q, :, ds(j * tile, tile)] = (g * jax.nn.sigmoid(g) * u).astype(BF16)
-            return carry
-
-        lax.fori_loop(0, len(order), first, 0)
+        order = [(0, 0), (0, 1), (0, 2), (0, 4), (1, 0), (1, 1), (0, 3), (1, 2), (1, 3), (1, 4)]
 
         def fold(i, q):
             landed(got.at[q, i], cr_r.at[q, i])
@@ -718,12 +669,12 @@
             def both(block, j):
                 return part[q, i, ds(block * own, own), :].astype(F32) + got[q, i, j].astype(F32)
 
-            @pl.when(q * (1 - i % 2) + 1 - q > 0)
+            @pl.when(jnp.logical_or(q == 0, straight(i) == 0))
             def _():
                 xsend[q, i] = both(tx, 1 - chip).astype(BF16)
                 xo(q, i).start()
 
-            @pl.when(q * (i % 2) > 0)
+            @pl.when(jnp.logical_and(q == 1, straight(i) == 1))
             def _():
                 esend[i, 1] = both(tx, 1 - chip).astype(BF16)
                 eo(i, 1).start()
@@ -736,62 +687,125 @@
             esend[i, 0] = (mixed + xgot[1, i].astype(F32)).astype(BF16)
             eo(i, 0).start()
 
-        def second(s, carry):
-            i, q = s // 2, 1 - s % 2
-
-            @pl.when(s == 0)
-            def _():
-                relay_dn(oe, 0, 1, grp=1 - side)
-
-            @pl.when(s == 4)
-            def _():
-                take_dn(o, 1 - side, 0)
-
-            @pl.when(s == 5)
-            def _():
-                relay_dn(oe, 1, 0, grp=1 - side)
-
-            @pl.when(s == 6)
-            def _():
-                take_dn(e, 1 - side, 0)
-
-            @pl.when(s == 8)
-            def _():
-                take_dn(oe, 1 - side, 0)
-
-            @pl.when(s == 10)
-            def _():
-                relay_dn(oe, 1, 1, grp=1 - side)
-                fold(4, 1)
-                fold(4, 0)
-                push(2)
-                take_dn(e, 1 - side, 1)
-
-            @pl.when(s == 12)
-            def _():
-                take_dn(oe, 1 - side, 1)
-
-            @pl.when(s == 14)
-            def _():
-                take_dn(o, side, 1)
-                take_dn(o, 1 - side, 1)
-
+        def product(q, i):
             weight = wd[pick(i, sources), pick(i, sides)]
             part[q, i] = jnp.dot(hid[q], weight, preferred_element_type=F32).astype(BF16)
             for j in range(2):
                 cr(q, i, j).start()
 
-            @pl.when(((s > 1) & (s < 10)) | (s > 11))
-            def _():
-                fold(i - 1, q)
-
-            @pl.when((s == 9) | (s == 12))
-            def _():
-                push(pick(s - 9, (0, 4, 4, 4)))
-
+        def first(i, carry):
+            q, j = pick(i, [a for a, _ in order]), pick(i, [b for _, b in order])
+
+            @pl.when(i == 0)
+            def _():
+                gathered(0)
+
+            @pl.when(i == 1)
+            def _():
+                relay_hosted(1)
+                relay_gu(oe, 3, grp=1 - side)
+                pass_hosted(0)
+
+            @pl.when(i == 2)
+            def _():
+                relay_gu(oe, 4, grp=1 - side)
+                send_gu(e, side, PIECES - 2, again=True, grp=1 - side)
+
+            @pl.when(i == 4)
+            def _():
+                pass_hosted(1)
+                for r in range(2):
+                    relay_dn(o, 0, r, grp=1 - side)
+                gathered(1)
+
+            @pl.when(i == 5)
+            def _():
+                relay_dn(e, 0, 0, sp=o)
+
+            @pl.when(i == 6)
+            def _():
+                relay_dn(e, 0, 1, sp=o)
+
+            @pl.when(i == 7)
+            def _():
+                for c in range(2):
+                    product(0, c)
+                relay_dn(e, 1, 0, sp=o)
+
+            @pl.when(i == 8)
+            def _():
+                relay_dn(oe, 0, 0, grp=1 - side)
+                relay_dn(e, 1, 1, sp=o)
+                send_dn(1 - side, 1, sp=o)
+                for c in range(2):
+                    fold(c, 0)
+
+            @pl.when(i == 9)
+            def _():
+                relay_dn(oe, 0, 1, grp=1 - side)
+
+            @pl.when(q == 0)
+            def _():
+                for source in (o, oe, e):
+                    take_gu(source, 1 - side, j)
+
+            g = jnp.dot(acts[q], wgu[0, j], preferred_element_type=F32)
+            u = jnp.dot(acts[q], wgu[1, j], preferred_element_type=F32)
+            hid[q, :, ds(j * tile, tile)] = (g * jax.nn.sigmoid(g) * u).astype(BF16)
             return carry
 
-        lax.fori_loop(0, 2 * chunks, second, 0)
+        lax.fori_loop(0, len(order), first, 0)
+
+        steps = [(1, 0), (1, 1)] + [(q, c) for c in range(2, chunks) for q in (1, 0)]
+
+        def step(s):
+            return pick(s, [a for a, _ in steps]), pick(s, [b for _, b in steps])
+
+        def second(s, carry):
+            q, i = step(s)
+
+            @pl.when(s == 2)
+            def _():
+                take_dn(o, 1 - side, 0)
+
+            @pl.when(s == 4)
+            def _():
+                relay_dn(oe, 1, 0, grp=1 - side)
+                take_dn(e, 1 - side, 0)
+
+            @pl.when(s == 6)
+            def _():
+                take_dn(oe, 1 - side, 0)
+
+            @pl.when(s == 8)
+            def _():
+                relay_dn(oe, 1, 1, grp=1 - side)
+                fold(4, 1)
+                fold(4, 0)
+                take_dn(e, 1 - side, 1)
+
+            @pl.when(s == 10)
+            def _():
+                take_dn(oe, 1 - side, 1)
+
+            @pl.when(s == 12)
+            def _():
+                take_dn(o, side, 1)
+                take_dn(o, 1 - side, 1)
+
+            product(q, i)
+
+            @pl.when(((s > 1) & (s < 8)) | (s > 9))
+            def _():
+                fold(*reversed(step(s - 2)))
+
+            @pl.when((s == 9) | (s == 10) | (s == 13))
+            def _():
+                push(pick(s - 9, (2, 3, 4, 4, 4)))
+
+            return carry
+
+        lax.fori_loop(0, len(steps), second, 0)
         for q in (1, 0):
             fold(chunks - 1, q)
         push(chunks - 2)
@@ -814,9 +828,9 @@
                 sent(acts.at[q, ds(me * own, own), :], ag_s.at[q, kind])
             sent(got.at[q], cr_s.at[q])
         sent(xsend.at[0], xo_s.at[0])
-        sent(xsend.at[1, : chunks // 2], xo_s.at[1])
+        sent(xsend.at[1, : chunks - len(whole)], xo_s.at[1])
         sent(esend.at[:, 0], eo_s.at[0])
-        sent(esend.at[: chunks // 2, 1], eo_s.at[1])
+        sent(esend.at[: len(whole), 1], eo_s.at[1])
 
     @pl.when(outer)
     def _():
@@ -831,26 +845,26 @@
         def finish(i):
             eo(i, 0).wait_recv()
             total = egot[0, i].astype(F32)
-            if i % 2:
+            if direct[i]:
                 er(i).wait_recv()
                 total += egot[1, i].astype(F32)
             at = ds((2 * sources[i] + sides[i]) * dw, dw)
             out_ref[:, at] = (mid[:, at].astype(F32) + 0.5 * total).astype(BF16)
 
-        for i in range(1, chunks, 2):
-            eo(i, 1).wait_recv()
-            er(i).start()
+        for i in range(chunks):
+            if direct[i]:
+                eo(i, 1).wait_recv()
+                er(i).start()
             if i > 1:
                 finish(i - 2)
-                finish(i - 3)
+        finish(chunks - 2)
         finish(chunks - 1)
-        finish(chunks - 2)
         sent(acts.at[0, ds(me * own, own), :], ea_s.at[0])
         sent_gu(place, side, 0, PIECES)
         sent_gu(place, 1 - side, 0, PIECES - 2)
         for half in (side, 1 - side):
             sent_dn(place, half, 0, 2)
-        sent(erelay.at[: chunks // 2], er_s.at[0])
+        sent(erelay.at[: len(whole)], er_s.at[0])
 
     for k in range(1, count):
 

time: 126 us -> 130 us (1.032)
  Pallas kernels: 124 us -> 129 us
    pallas_call x1, Pallas kernels: 124 us -> 129 us  [fast_body(): pl.pallas_call(layer_kernel, out_shape=pltpu.MemorySpace.VMEM((own, model...]
where the time goes in v4:
time: 130 us
  Pallas kernels  129 us (99%)
    pallas_call x1, Pallas kernels, fast_body(): pl.pallas_call(layer_kernel, out_shape=pltpu.MemorySpace.VMEM((own, model...  129 us

profile of v4, /device:TPU:0, one launch (start us, length us, event | category | flops | bytes accessed | tf_op | source)
XLA Modules:
  0.0 129.8 jit_solution(9748401931798354936)
XLA Ops:
  0.0 128.9 %layer.1 = bf16[192,2048]{1,0:T(8,128)(2,1)S(1)} custom-call(bf16[768,128]{1,0:T(8,128)(2,1)} %k_hbm.1, bf16[768,256]{1,0:T(8,128)(2,1)} %v_hbm.1, bf16[768,128]{1,0:T(8,128)(2,1)} %fd_hbm.1, bf16[768,128]{1,0:T(8,128)(2,1)} %bd_hbm.1, f32[2,128]{1,0:T(2,128)} %shift_hbm.1, f32[2,768]{1,0:T(2,128)} %spike_hbm.1, bf16[768,128]{1,0:T(8,128)(2,1)} %q_hbm.1, ...), custom_call_target="tpu_custom_call" | custom-call | flops 30000001024 | bytes 30000000 | tf_op jit(solution)/shard_map/layer/pallas_call | solution.py:976
  129.0 0.9 copy.17

commit v5 on v4

--- a/solution.py
+++ b/solution.py
@@ -349,9 +349,9 @@
     res_hbm, out_hbm, g_hbm, u_hbm, d_hbm,
     out_ref,
     k_ref, v_ref, fd_ref, bd_ref, shift_ref, spike_ref, q_ref, gate_ref, gain_ref, norm_ref, in_s,
-    within, kd, fown, bown, fgot, bgot, fstate, bstate, held, attended, rows, outw, res, mid, acts,
+    within, kd, fown, bown, fgot, bgot, fstate, bstate, held, attended, rows, outl, outh, pout, rgot, rxs, rxg, squares, res, mid, acts,
     wgu, wd, hid, part, got, xsend, xgot, esend, egot, erelay,
-    loc, st_s, st_r, a2a_s, a2a_r, ow_s, ow_r, ag_s, ag_r, ea_s, ea_r, gs, gr, dsd, drv, cr_s, cr_r, xo_s, xo_r,
+    loc, st_s, st_r, a2a_s, a2a_r, ow_s, ow_r, rs_s, rs_r, rx_s, rx_r, ag_s, ag_r, ea_s, ea_r, gs, gr, dsd, drv, cr_s, cr_r, xo_s, xo_r,
     eo_s, eo_r, er_s, er_r,
 ):
     count = lax.axis_size("sp")
@@ -371,7 +371,8 @@
     dr = hidden // 2
     dw = wd.shape[3]
     chunks = part.shape[1]
-    orow = width // 4
+    wide = pout.shape[2]
+    parts = pout.shape[0]
     nrow = own // 2
 
     def remote(src, dst, send, recv, **dev):
@@ -385,10 +386,11 @@
         send = gs.at[source, 1 - half if again else half]
         return remote(src, dst, send, gr.at[n, source, half, p], **(dev or dict(sp=o)))
 
-    def dn(source, half, p, r, local=False, **dev):
+    def dn(source, half, p, r, local=False, again=False, **dev):
         dst = wd.at[source, p, ds(half * dr + r * (dr // 2), dr // 2), :]
         src = d_hbm.at[ds(half * dr + r * (dr // 2), dr // 2), p * dw : (p + 1) * dw] if local else dst
-        return remote(src, dst, dsd.at[source, half], drv.at[source, half, p, r], **(dev or dict(sp=o)))
+        send = dsd.at[source, 1 - half if again else half]
+        return remote(src, dst, send, drv.at[source, half, p, r], **(dev or dict(sp=o)))
 
     def send_gu(source, half, p, local=False, again=False, **dev):
         for n in range(2):
@@ -429,18 +431,25 @@
         remote(ref, ref, sem, sem, sp=o).wait_recv()
 
     def ow(kind, block, i, dev, local=False):
-        dst = outw.at[ds(block * width + i * orow, orow), :]
-        src = out_hbm.at[i * orow : (i + 1) * orow, :] if local else dst
-        return remote(src, dst, ow_s.at[kind], ow_r.at[i if kind == 0 else 3 + kind], tp=dev)
+        half = width // 2
+        dst = outh.at[ds(block * width + i * half, half), :]
+        src = out_hbm.at[i * half : (i + 1) * half, model // 2 :] if local else dst
+        return remote(src, dst, ow_s.at[kind], ow_r.at[i if kind == 0 else 1 + kind], tp=dev)
 
     def relay_ow(i):
         ow(0, tx, i, tc).wait_recv()
         ow(2, tx, i, tc).start()
 
-    def a2a(n, block, dev):
-        return remote(
-            attended.at[ds(dev * own, own), :], rows.at[:, ds(block * width, width)], a2a_s.at[n], a2a_r.at[block], tp=dev
-        )
+    def a2a(block, dev):
+        src = attended.at[ds(dev * own, own), :]
+        return remote(src, rows.at[:, ds(block * width, width)], a2a_s.at[0], a2a_r.at[block], tp=dev)
+
+    def rs(c, j):
+        block = 2 * j + 1 - core
+        return remote(pout.at[c, ds(block * own, own), :], rgot.at[c, j], rs_s.at[0], rs_r.at[c], tp=tc)
+
+    def rx(c):
+        return remote(rxs.at[c], rxg.at[c], rx_s.at[0], rx_r.at[c], tp=tx)
 
     def ag(q, kind, block, i, dev):
         at = acts.at[q, ds(block * own + i * nrow, nrow), :]
@@ -489,7 +498,8 @@
         pltpu.make_async_copy(own_gu, own_gu, loc.at[0]),
         pltpu.make_async_copy(wd.at[place], wd.at[place], loc.at[1]),
     ]
-    own_out = pltpu.make_async_copy(out_hbm, outw.at[ds(me * width, width), :], loc.at[2])
+    own_low = pltpu.make_async_copy(out_hbm.at[:, : model // 2], outl, loc.at[2])
+    own_high = pltpu.make_async_copy(out_hbm.at[:, model // 2 :], outh.at[ds(me * width, width), :], loc.at[4])
     own_res = pltpu.make_async_copy(res_hbm, res, loc.at[3])
 
     barrier = pltpu.get_barrier_semaphore()
@@ -516,23 +526,13 @@
     ]
     for load in loads:
         load.start()
-    pl.semaphore_wait(barrier, len(friends))
-
-    @pl.when(middle)
-    def _():
-        gu(0, place, side, 0, True, sp=o).start()
-
-    @pl.when(outer)
-    def _():
-        gu(0, place, side, 0, True, sp=m).start()
-
-    for i in range(4):
-        ow(0, me, i, tx, True).start()
-    for i in range(4):
-        ow(1, me, i, tc, True).start()
+    own_low.start()
+    own_high.start()
+    own_res.start()
     for load in loads[:6]:
         load.wait()
     own_states(k_ref, v_ref, fd_ref, bd_ref, shift_ref, spike_ref, within, kd, fown, bown)
+    pl.semaphore_wait(barrier, len(friends))
 
     for k in range(1, count):
 
@@ -546,19 +546,17 @@
 
     @pl.when(middle)
     def _():
-        gu(1, place, side, 0, True, sp=o).start()
-        for p in range(1, PIECES):
+        for p in range(PIECES):
             send_gu(place, side, p, True, sp=o)
 
     @pl.when(outer)
     def _():
-        gu(1, place, side, 0, True, sp=m).start()
-        for p in range(1, PIECES):
+        for p in range(PIECES):
             send_gu(place, side, p, True, sp=m)
-        send_gu(place, 1 - side, 0, True, sp=m)
-
-    own_out.start()
-    own_res.start()
+
+    for i in range(2):
+        ow(0, me, i, tx, True).start()
+        ow(1, me, i, tc, True).start()
 
     @pl.when(middle)
     def _():
@@ -586,58 +584,88 @@
     backward_states(k_ref, v_ref, within, bstate[...], held)
     attend(q_ref, k_ref, v_ref, within, gate_ref, gain_ref, fstate[...], held, attended)
     others = (tx, td, tc)
-    for n, t in enumerate(others):
-        a2a(n, me, t).start()
+    for t in others:
+        a2a(me, t).start()
     rows[:, ds(me * width, width)] = attended[ds(me * own, own), :]
-
-    for p in range(4):
-        relay_ow(p)
-
-        @pl.when(middle)
-        def _(p=p):
-            relay_gu(o, p, grp=1 - side)
-            relay_gu(e, p, sp=o)
-
-    for t in others:
-        a2a(0, t, t).wait_recv()
-    for kind, t in ((1, tc), (2, td)):
-        landed(outw.at[ds(t * width, width), :], ow_r.at[3 + kind])
-    own_out.wait()
-    own_res.wait()
-
-    total = jnp.zeros((own, 1), F32)
-    wide = 512
-    for n in range(model // wide):
-        at = slice(n * wide, (n + 1) * wide)
-        projected = jnp.dot(rows[...], outw[:, at], preferred_element_type=F32)
+    own_low.wait()
+    for c in range(parts):
+        at = slice(c * wide, (c + 1) * wide)
+        pout[c] = jnp.dot(attended[...], outl[:, at], preferred_element_type=F32).astype(BF16)
+        for j in range(2):
+            rs(c, j).start()
+    relay_ow(0)
+    for c in range(parts):
+        landed(rgot.at[c], rs_r.at[c])
+        rxs[c] = (pout[c, ds(tx * own, own), :].astype(F32) + rgot[c, 1 - chip].astype(F32)).astype(BF16)
+        rx(c).start()
+
+    def mix(at, projected):
         mixed = (res[:, at].astype(F32) + projected).astype(BF16)
         mid[:, at] = mixed
         mixed = mixed.astype(F32)
-        total += jnp.sum(mixed * mixed, axis=-1, keepdims=True)
+        return jnp.sum(mixed * mixed, axis=-1, keepdims=True)
+
+    @pl.when(middle)
+    def _():
+        relay_gu(o, 0, grp=1 - side)
+        relay_gu(e, 0, sp=o)
+
+    relay_ow(1)
+
+    @pl.when(middle)
+    def _():
+        relay_gu(o, 1, grp=1 - side)
+        relay_gu(e, 1, sp=o)
+
+    for t in others:
+        a2a(t, t).wait_recv()
+    for kind, t in ((1, tc), (2, td)):
+        landed(outh.at[ds(t * width, width), :], ow_r.at[1 + kind])
+    own_high.wait()
+    own_res.wait()
+    total = jnp.zeros((own, 1), F32)
+    for n in range(parts):
+        high = slice(n * wide, (n + 1) * wide)
+        projected = jnp.dot(rows[...], outh[:, high], preferred_element_type=F32)
+        total += mix(slice(model // 2 + n * wide, model // 2 + (n + 1) * wide), projected)
+    squares[...] = jnp.broadcast_to(total, squares.shape)
+
+    @pl.when(middle)
+    def _():
+        relay_gu(o, 2, grp=1 - side)
+        relay_gu(e, 2, sp=o)
+
+    total = squares[:, :1]
+    for n in range(parts):
+        rx(n).wait_recv()
+        projected = pout[n, ds(me * own, own), :].astype(F32) + rgot[n, chip].astype(F32) + rxg[n].astype(F32)
+        total += mix(slice(n * wide, (n + 1) * wide), projected)
     inverse = lax.rsqrt(total / model + EPSILON)
-    for n in range(model // wide):
+    for n in range(2 * parts):
         at = slice(n * wide, (n + 1) * wide)
         acts[0, ds(me * own, own), at] = (mid[:, at].astype(F32) * inverse * norm_ref[:, at]).astype(BF16)
 
-    direct = (1, 1, 0, 0, 0, 1, 0, 1)
+    direct = (1, 1, 1, 0, 0, 0, 0, 1)
     whole = [i for i, d in enumerate(direct) if d]
 
     def straight(i):
         return direct[i] if isinstance(i, int) else pick(i, direct)
 
-    sources = (m, m, o, e, oe, e, oe, o)
-    sides = (0, 1, 0, 0, 0, 1, 1, 1)
+    sources = (m, m, o, o, e, oe, e, oe)
+    sides = (0, 1, 0, 1, 0, 0, 1, 1)
 
     @pl.when(middle)
     def _():
         for i in range(2):
             ag(0, 0, me, i, tx).start()
             ag(0, 1, me, i, tc).start()
-        relay_gu(o, 4, grp=1 - side)
-        relay_gu(e, 4, sp=o)
-        send_gu(e, side, PIECES - 1, again=True, grp=1 - side)
+        for p in range(3, PIECES):
+            relay_gu(o, p, grp=1 - side)
+            relay_gu(e, p, sp=o)
+        send_gu(e, side, 1, again=True, grp=1 - side)
         for p in range(2):
             send_dn(side, p, sp=o)
+        send_dn(1 - side, 1, sp=o)
         for copy in own_waits:
             copy.wait()
 
@@ -656,12 +684,13 @@
 
         relay_gu(oe, 0, grp=1 - side)
         relay_own(0)
+        relay_hosted(0)
         relay_gu(oe, 1, grp=1 - side)
-        relay_hosted(0)
+        relay_own(1)
         relay_gu(oe, 2, grp=1 - side)
-        relay_own(1)
-
-        order = [(0, 0), (0, 1), (0, 2), (0, 4), (1, 0), (1, 1), (0, 3), (1, 2), (1, 3), (1, 4)]
+        relay_hosted(1)
+
+        order = [(0, 0), (0, 1), (0, 2), (1, 0), (1, 1), (0, 3), (1, 2), (1, 3), (0, 4), (1, 4)]
 
         def fold(i, q):
             landed(got.at[q, i], cr_r.at[q, i])
@@ -682,6 +711,8 @@
                 eo(i, 0).start()
 
         def push(i):
+            if direct[i]:
+                return
             xo(1, i).wait_recv()
             mixed = part[1, i, ds(me * own, own), :].astype(F32) + got[1, i, chip].astype(F32)
             esend[i, 0] = (mixed + xgot[1, i].astype(F32)).astype(BF16)
@@ -702,47 +733,26 @@
 
             @pl.when(i == 1)
             def _():
-                relay_hosted(1)
+                pass_hosted(0)
                 relay_gu(oe, 3, grp=1 - side)
-                pass_hosted(0)
 
             @pl.when(i == 2)
             def _():
                 relay_gu(oe, 4, grp=1 - side)
-                send_gu(e, side, PIECES - 2, again=True, grp=1 - side)
-
-            @pl.when(i == 4)
-            def _():
                 pass_hosted(1)
+
+            @pl.when(i == 3)
+            def _():
+                gathered(1)
+
+            @pl.when(i == 5)
+            def _():
                 for r in range(2):
                     relay_dn(o, 0, r, grp=1 - side)
-                gathered(1)
-
-            @pl.when(i == 5)
+
+            @pl.when(i == 9)
             def _():
                 relay_dn(e, 0, 0, sp=o)
-
-            @pl.when(i == 6)
-            def _():
-                relay_dn(e, 0, 1, sp=o)
-
-            @pl.when(i == 7)
-            def _():
-                for c in range(2):
-                    product(0, c)
-                relay_dn(e, 1, 0, sp=o)
-
-            @pl.when(i == 8)
-            def _():
-                relay_dn(oe, 0, 0, grp=1 - side)
-                relay_dn(e, 1, 1, sp=o)
-                send_dn(1 - side, 1, sp=o)
-                for c in range(2):
-                    fold(c, 0)
-
-            @pl.when(i == 9)
-            def _():
-                relay_dn(oe, 0, 1, grp=1 - side)
 
             @pl.when(q == 0)
             def _():
@@ -756,58 +766,71 @@
 
         lax.fori_loop(0, len(order), first, 0)
 
-        steps = [(1, 0), (1, 1)] + [(q, c) for c in range(2, chunks) for q in (1, 0)]
-
-        def step(s):
-            return pick(s, [a for a, _ in steps]), pick(s, [b for _, b in steps])
-
         def second(s, carry):
-            q, i = step(s)
-
-            @pl.when(s == 2)
+            i, q = s // 2, 1 - s % 2
+
+            @pl.when(s == 0)
+            def _():
+                relay_dn(e, 0, 1, sp=o)
+                dn(e, side, 0, 1, again=True, grp=1 - side).start()
+
+            @pl.when(s == 4)
             def _():
                 take_dn(o, 1 - side, 0)
 
-            @pl.when(s == 4)
-            def _():
-                relay_dn(oe, 1, 0, grp=1 - side)
+            @pl.when(s == 5)
+            def _():
+                relay_dn(e, 1, 0, sp=o)
+
+            @pl.when(s == 6)
+            def _():
+                take_dn(o, side, 1)
+                take_dn(o, 1 - side, 1)
+
+            @pl.when(s == 8)
+            def _():
+                relay_dn(oe, 0, 0, grp=1 - side)
+                fold(3, 1)
+                relay_dn(e, 1, 1, sp=o)
+                fold(3, 0)
+                relay_dn(oe, 0, 1, grp=1 - side)
+                push(2)
                 take_dn(e, 1 - side, 0)
 
-            @pl.when(s == 6)
-            def _():
-                take_dn(oe, 1 - side, 0)
-
-            @pl.when(s == 8)
-            def _():
-                relay_dn(oe, 1, 1, grp=1 - side)
+            @pl.when(s == 10)
+            def _():
                 fold(4, 1)
                 fold(4, 0)
+                push(3)
+                relay_dn(oe, 1, 0, grp=1 - side)
+                take_dn(oe, 1 - side, 0)
+
+            @pl.when(s == 12)
+            def _():
+                fold(5, 1)
+                relay_dn(oe, 1, 1, grp=1 - side)
+                fold(5, 0)
+                push(4)
                 take_dn(e, 1 - side, 1)
 
-            @pl.when(s == 10)
-            def _():
+            @pl.when(s == 14)
+            def _():
+                fold(6, 1)
+                fold(6, 0)
+                push(5)
                 take_dn(oe, 1 - side, 1)
 
-            @pl.when(s == 12)
-            def _():
-                take_dn(o, side, 1)
-                take_dn(o, 1 - side, 1)
-
             product(q, i)
 
-            @pl.when(((s > 1) & (s < 8)) | (s > 9))
-            def _():
-                fold(*reversed(step(s - 2)))
-
-            @pl.when((s == 9) | (s == 10) | (s == 13))
-            def _():
-                push(pick(s - 9, (2, 3, 4, 4, 4)))
+            @pl.when((s > 1) & (s < 8))
+            def _():
+                fold(i - 1, q)
 
             return carry
 
-        lax.fori_loop(0, len(steps), second, 0)
-        for q in (1, 0):
-            fold(chunks - 1, q)
+        lax.fori_loop(0, 2 * chunks, second, 0)
+        fold(chunks - 1, 1)
+        fold(chunks - 1, 0)
         push(chunks - 2)
 
         for i in range(chunks):
@@ -818,7 +841,8 @@
 
         for source in (place, e, o, oe):
             sent_gu(source, side, 0, PIECES)
-        sent_gu(e, side, PIECES - 2, PIECES, again=True)
+        sent_gu(e, side, 0, 1, again=True)
+        sent(wd.at[e, 0, : dr // 2, :], dsd.at[e, 1 - side])
         for source in (place, e, oe):
             sent_dn(source, side, 0, 2)
         sent_dn(o, side, 0, 1)
@@ -836,11 +860,12 @@
     def _():
         for i in range(2):
             to_host(i).start()
-        for p in range(1, PIECES - 2):
+        for p in (0, 2, 3, 4):
             send_gu(place, 1 - side, p, True, sp=m)
-        for half in (side, 1 - side):
-            for p in range(2):
-                send_dn(half, p, sp=m)
+        for p in range(2):
+            send_dn(side, p, sp=m)
+        dn(place, 1 - side, 0, 0, True, sp=m).start()
+        send_dn(1 - side, 1, sp=m)
 
         def finish(i):
             eo(i, 0).wait_recv()
@@ -861,9 +886,9 @@
         finish(chunks - 1)
         sent(acts.at[0, ds(me * own, own), :], ea_s.at[0])
         sent_gu(place, side, 0, PIECES)
-        sent_gu(place, 1 - side, 0, PIECES - 2)
-        for half in (side, 1 - side):
-            sent_dn(place, half, 0, 2)
+        sent_gu(place, 1 - side, 0, PIECES - 1)
+        sent_dn(place, side, 0, 2)
+        sent(wd.at[place, 0, : dr + dr // 2, :], dsd.at[place, 1 - side])
         sent(erelay.at[: len(whole)], er_s.at[0])
 
     for k in range(1, count):
@@ -876,10 +901,11 @@
         def _(k=k):
             state_copy(1, k, place).wait_send()
 
-    for n, t in enumerate(others):
-        a2a(n, me, t).wait_send()
+    sent(rows.at[:, : 3 * width], a2a_s.at[0])
     for kind in range(3):
-        sent(outw.at[ds(me * width, width), :], ow_s.at[kind])
+        sent(outh.at[ds(me * width, width), :], ow_s.at[kind])
+    sent(rgot, rs_s.at[0])
+    sent(rxs, rx_s.at[0])
 
 
 def fast_body(
@@ -906,7 +932,6 @@
     depth, hidden = gate_projection.shape
     dw = down_projection.shape[1] // 2
     chunks = 2 * count
-    tps = tokens // own
     blocks = tokens // BLOCK
     dma = lambda *shape: pltpu.SemaphoreType.DMA(shape)
     state = (HEAD_V + 16, lanes)
@@ -933,8 +958,14 @@
         V((HEAD_V, lanes), F32),
         V((blocks, 2 * HEAD_V, lanes), BF16),
         V((tokens, width), BF16),
-        V((own, tps * width), BF16),
-        V((tps * width, model), BF16),
+        V((own, tokens // own * width), BF16),
+        V((width, model // 2), BF16),
+        V((tokens // own * width, model // 2), BF16),
+        V((2, tokens, model // 4), BF16),
+        V((2, 2, own, model // 4), BF16),
+        V((2, own, model // 4), BF16),
+        V((2, own, model // 4), BF16),
+        V((own, 128), F32),
         V((own, model), BF16),
         V((own, model), BF16),
         V((2, tokens, model), BF16),
@@ -948,13 +979,17 @@
         V((chunks, 2, own, dw), BF16),
         V((2, chunks, own, dw), BF16),
         V((chunks, own, dw), BF16),
-        dma(4),
+        dma(5),
         dma(2, count - 1),
         dma(2, count - 1),
+        dma(1),
+        dma(tokens // own),
         dma(3),
-        dma(tps),
-        dma(3),
-        dma(6),
+        dma(4),
+        dma(1),
+        dma(2),
+        dma(1),
+        dma(2),
         dma(2, 3),
         dma(2, 4),
         dma(1),

time: 130 us -> 122 us (0.938)
  Pallas kernels: 129 us -> 121 us
    pallas_call x1, Pallas kernels: 129 us -> 121 us  [fast_body(): pl.pallas_call(layer_kernel, out_shape=pltpu.MemorySpace.VMEM((own, model...]
where the time goes in v5:
time: 122 us; the launch traced here: 121 us
  Pallas kernels  121 us (99%)
    pallas_call x1, Pallas kernels, fast_body(): pl.pallas_call(layer_kernel, out_shape=pltpu.MemorySpace.VMEM((own, model...  121 us

profile of v5, /device:TPU:0, one launch (start us, length us, event | category | flops | bytes accessed | tf_op | source)
XLA Modules:
  0.0 121.5 jit_solution(9206443800056438670)
XLA Ops:
  0.0 120.6 %layer.1 = bf16[192,2048]{1,0:T(8,128)(2,1)S(1)} custom-call(bf16[768,128]{1,0:T(8,128)(2,1)} %k_hbm.1, bf16[768,256]{1,0:T(8,128)(2,1)} %v_hbm.1, bf16[768,128]{1,0:T(8,128)(2,1)} %fd_hbm.1, bf16[768,128]{1,0:T(8,128)(2,1)} %bd_hbm.1, f32[2,128]{1,0:T(2,128)} %shift_hbm.1, f32[2,768]{1,0:T(2,128)} %spike_hbm.1, bf16[768,128]{1,0:T(8,128)(2,1)} %q_hbm.1, ...), custom_call_target="tpu_custom_call" | custom-call | flops 30000001024 | bytes 30000000 | tf_op jit(solution)/shard_map/layer/pallas_call | solution.py:1011
  120.6 0.9 copy.17

commit v6 on v5

--- a/solution.py
+++ b/solution.py
@@ -380,17 +380,20 @@
             src_ref=src, dst_ref=dst, send_sem=send, recv_sem=recv, device_id=dev, device_id_type=MESH
         )
 
+    def slot(source, dev):
+        return source - jnp.where(source > dev.get("sp", place), 1, 0)
+
     def gu(n, source, half, p, local=False, again=False, **dev):
         dst = wgu.at[n, p, ds(source * depth + half * hr, hr), :]
         src = (g_hbm, u_hbm)[n].at[ds(half * hr, hr), ds(p * tile, tile)] if local else dst
         send = gs.at[source, 1 - half if again else half]
-        return remote(src, dst, send, gr.at[n, source, half, p], **(dev or dict(sp=o)))
+        return remote(src, dst, send, gr.at[n, slot(source, dev), half, p], **(dev or dict(sp=o)))
 
     def dn(source, half, p, r, local=False, again=False, **dev):
         dst = wd.at[source, p, ds(half * dr + r * (dr // 2), dr // 2), :]
         src = d_hbm.at[ds(half * dr + r * (dr // 2), dr // 2), p * dw : (p + 1) * dw] if local else dst
         send = dsd.at[source, 1 - half if again else half]
-        return remote(src, dst, send, drv.at[source, half, p, r], **(dev or dict(sp=o)))
+        return remote(src, dst, send, drv.at[slot(source, dev), half, p, r], **(dev or dict(sp=o)))
 
     def send_gu(source, half, p, local=False, again=False, **dev):
         for n in range(2):
@@ -400,10 +403,13 @@
         for n in range(2):
             gu(n, source, half, p).wait_recv()
 
+    def relay_one(n, source, p, **dev):
+        gu(n, source, side, p).wait_recv()
+        gu(n, source, side, p, **dev).start()
+
     def relay_gu(source, p, **dev):
         for n in range(2):
-            gu(n, source, side, p).wait_recv()
-            gu(n, source, side, p, **dev).start()
+            relay_one(n, source, p, **dev)
 
     def send_dn(half, p, **dev):
         for r in range(2):
@@ -593,6 +599,10 @@
         pout[c] = jnp.dot(attended[...], outl[:, at], preferred_element_type=F32).astype(BF16)
         for j in range(2):
             rs(c, j).start()
+    @pl.when(middle)
+    def _():
+        relay_one(0, o, 0, grp=1 - side)
+
     relay_ow(0)
     for c in range(parts):
         landed(rgot.at[c], rs_r.at[c])
@@ -607,7 +617,7 @@
 
     @pl.when(middle)
     def _():
-        relay_gu(o, 0, grp=1 - side)
+        relay_one(1, o, 0, grp=1 - side)
         relay_gu(e, 0, sp=o)
 
     relay_ow(1)
@@ -690,7 +700,7 @@
         relay_gu(oe, 2, grp=1 - side)
         relay_hosted(1)
 
-        order = [(0, 0), (0, 1), (0, 2), (1, 0), (1, 1), (0, 3), (1, 2), (1, 3), (0, 4), (1, 4)]
+        order = [(0, 0), (0, 1), (0, 2), (1, 0), (0, 3), (1, 1), (1, 2), (1, 3), (0, 4), (1, 4)]
 
         def fold(i, q):
             landed(got.at[q, i], cr_r.at[q, i])
@@ -799,32 +809,30 @@
 
             @pl.when(s == 10)
             def _():
+                push(3)
+                relay_dn(oe, 1, 0, grp=1 - side)
                 fold(4, 1)
                 fold(4, 0)
-                push(3)
-                relay_dn(oe, 1, 0, grp=1 - side)
                 take_dn(oe, 1 - side, 0)
 
             @pl.when(s == 12)
             def _():
+                relay_dn(oe, 1, 1, grp=1 - side)
                 fold(5, 1)
-                relay_dn(oe, 1, 1, grp=1 - side)
-                fold(5, 0)
                 push(4)
                 take_dn(e, 1 - side, 1)
 
             @pl.when(s == 14)
             def _():
                 fold(6, 1)
-                fold(6, 0)
                 push(5)
                 take_dn(oe, 1 - side, 1)
 
             product(q, i)
 
-            @pl.when((s > 1) & (s < 8))
-            def _():
-                fold(i - 1, q)
+            @pl.when(((s > 1) & (s < 8)) | (s == 12) | (s == 14))
+            def _():
+                fold(i - 1, jnp.where(s < 8, q, 0))
 
             return carry
 
@@ -995,9 +1003,9 @@
         dma(1),
         dma(2),
         dma(count, 2),
-        dma(2, count, 2, PIECES),
+        dma(2, count - 1, 2, PIECES),
         dma(count, 2),
-        dma(count, 2, 2, 2),
+        dma(count - 1, 2, 2, 2),
         dma(2),
         dma(2, chunks),
         dma(2),

time: 122 us -> 121 us (level)
  no operation moved by 1% of the time
where the time goes in v6:
time: 121 us
  Pallas kernels  120 us (99%)
    pallas_call x1, Pallas kernels, fast_body(): pl.pallas_call(layer_kernel, out_shape=pltpu.MemorySpace.VMEM((own, model...  120 us

profile of v6, /device:TPU:0, one launch (start us, length us, event | category | flops | bytes accessed | tf_op | source)
XLA Modules:
  0.0 120.9 jit_solution(15167691338946685784)
XLA Ops:
  0.0 120.0 %layer.1 = bf16[192,2048]{1,0:T(8,128)(2,1)S(1)} custom-call(bf16[768,128]{1,0:T(8,128)(2,1)} %k_hbm.1, bf16[768,256]{1,0:T(8,128)(2,1)} %v_hbm.1, bf16[768,128]{1,0:T(8,128)(2,1)} %fd_hbm.1, bf16[768,128]{1,0:T(8,128)(2,1)} %bd_hbm.1, f32[2,128]{1,0:T(2,128)} %shift_hbm.1, f32[2,768]{1,0:T(2,128)} %spike_hbm.1, bf16[768,128]{1,0:T(8,128)(2,1)} %q_hbm.1, ...), custom_call_target="tpu_custom_call" | custom-call | flops 30000001024 | bytes 30000000 | tf_op jit(solution)/shard_map/layer/pallas_call | solution.py:1019
  120.0 0.9 copy.17

commit v7 on v6

--- a/solution.py
+++ b/solution.py
@@ -830,14 +830,19 @@
 
             product(q, i)
 
-            @pl.when(((s > 1) & (s < 8)) | (s == 12) | (s == 14))
-            def _():
-                fold(i - 1, jnp.where(s < 8, q, 0))
+            @pl.when((s > 1) & (s < 8))
+            def _():
+                fold(i - 1, q)
+
+            @pl.when(s == 14)
+            def _():
+                fold(chunks - 3, 0)
 
             return carry
 
         lax.fori_loop(0, 2 * chunks, second, 0)
         fold(chunks - 1, 1)
+        fold(chunks - 2, 0)
         fold(chunks - 1, 0)
         push(chunks - 2)
 

time: 121 us -> 121 us (level)
  no operation moved by 1% of the time
where the time goes in v7:
time: 121 us
  Pallas kernels  120 us (99%)
    pallas_call x1, Pallas kernels, fast_body(): pl.pallas_call(layer_kernel, out_shape=pltpu.MemorySpace.VMEM((own, model...  120 us

profile of v7, /device:TPU:0, one launch (start us, length us, event | category | flops | bytes accessed | tf_op | source)
XLA Modules:
  0.0 120.8 jit_solution(16882754599362811177)
XLA Ops:
  0.0 119.9 %layer.1 = bf16[192,2048]{1,0:T(8,128)(2,1)S(1)} custom-call(bf16[768,128]{1,0:T(8,128)(2,1)} %k_hbm.1, bf16[768,256]{1,0:T(8,128)(2,1)} %v_hbm.1, bf16[768,128]{1,0:T(8,128)(2,1)} %fd_hbm.1, bf16[768,128]{1,0:T(8,128)(2,1)} %bd_hbm.1, f32[2,128]{1,0:T(2,128)} %shift_hbm.1, f32[2,768]{1,0:T(2,128)} %spike_hbm.1, bf16[768,128]{1,0:T(8,128)(2,1)} %q_hbm.1, ...), custom_call_target="tpu_custom_call" | custom-call | flops 30000001024 | bytes 30000000 | tf_op jit(solution)/shard_map/layer/pallas_call | solution.py:1024
  120.0 0.9 copy.17
